TPU v7x, 768 devices: a whole 4x8x12 slice. The times are simulated.
768 devices in a mesh: sp: 12 (over z), tp: 8 (over y), dp: 8 (over x, core).
Axes of the slice: x: 4, y: 8, z: 12, core: 2. Of those that a mesh axis runs over, the one named last changes fastest.
Arguments:
- latents: bfloat16 [8, 6144, 3072], P('dp', ('sp', 'tp')), may hold values from -5 to 5
- condition: bfloat16 [8, 3072], P('dp', ('sp', 'tp')), may hold values from -6 to 6
- context: bfloat16 [8, 384, 3072], P('dp', ('sp', 'tp')), may hold values from -6 to 6
- context_cond: bfloat16 [3072], P(('sp', 'tp')), may hold values from -6 to 6
- shift_weight: bfloat16 [3072, 3072], P(('sp', 'tp')), may hold values from -0.109375 to 0.109375
- scale_weight: bfloat16 [3072, 3072], P(('sp', 'tp')), may hold values from -0.109375 to 0.109375
- out_gate_weight: bfloat16 [3072, 3072], P(('sp', 'tp')), may hold values from -0.109375 to 0.109375
- pre_gain: float32 [3072], replicated, may hold values from 0.1 to 1.9
- post_gain: float32 [3072], replicated, may hold values from 0.1 to 1.9
- query_weight: bfloat16 [3072, 1024], P(None, 'tp'), may hold values from -0.108253175 to 0.108253175
- key_weight: bfloat16 [3072, 256], replicated, may hold values from -0.108253175 to 0.108253175
- value_weight: bfloat16 [3072, 256], replicated, may hold values from -0.109375 to 0.109375
- head_gate_weight: bfloat16 [3072, 1024], P(None, 'tp'), may hold values from -0.109375 to 0.109375
- lambdas: float32 [8], P('tp'), may hold values from 0.3 to 0.8
- head_gain: float32 [128], replicated, may hold values from 0.1 to 1.9
- out_weight: bfloat16 [1024, 3072], P(None, 'tp'), may hold values from -0.1875 to 0.1875
Outputs:
- mixed_out: bfloat16 [8, 6144, 3072], P('dp', ('sp', 'tp'))
All inputs are finite; a program needn't handle non-finite values.
Results may differ from a plain program's by a relative error of at most 0.0128.
The roundings to bfloat16 on the way count: a program that leaves them out, or rounds other values in their place, can miss the bound.
Values may be sent and summed in bfloat16 or wider, within the bound.
No kernel may reach another device: no remote copies, remote signals or barrier semaphores. Data moves between devices by JAX's collectives and lax.ppermute only.
A program may use at most 64 MiB of HBM per device.

v0:
```python
import math

import jax
import jax.numpy as jnp
from jax import lax
from jax.sharding import PartitionSpec as P

HEADS = 8
KVH = 2
HQK = 64
HV = 128


NORM_EPSILON = 1e-06


def over_axes(shard, axes):
    for axis in axes:
        shard = lax.psum(shard, axis)
    return shard


def in_one_piece(arrays, axis, dim, along):
    widths = [a.shape[along] for a in arrays]
    both = jnp.concatenate(arrays, axis=along)
    whole = lax.all_gather(both, axis, axis=dim, tiled=True)
    return tuple(jnp.split(whole, [sum(widths[:k]) for k in range(1, len(widths))], axis=along))


def copy_for_each(shard, axis):
    copies = jnp.broadcast_to(shard, (lax.axis_size(axis), *shard.shape))
    return lax.all_to_all(copies, axis, split_axis=0, concat_axis=0, tiled=True)


def laid_out(parts, dim):
    parts = jnp.moveaxis(parts, 0, dim)
    shape = parts.shape
    return parts.reshape(*shape[:dim], shape[dim] * shape[dim + 1], *shape[dim + 2 :])


def gathered_copies(shard, axis, dim):
    parts = copy_for_each(shard, axis)
    return laid_out(parts, dim)


def norm_rows(values, norm_gain):
    return (
        values
        * lax.rsqrt(jnp.mean(values * values, axis=-1, keepdims=True) + NORM_EPSILON)
        * norm_gain
    )


def modulate(tokens, norm_gain, shifts, scales):
    values = norm_rows(tokens.astype(jnp.float32), norm_gain)
    return (values * (1.0 + scales[:, None, :]) + shifts[:, None, :]).astype(jnp.bfloat16)


def project(tokens, weight):
    flattened = tokens.reshape(-1, tokens.shape[-1])
    result = jnp.dot(flattened, weight, preferred_element_type=jnp.float32).astype(jnp.bfloat16)
    return result.reshape(tokens.shape[:-1] + (weight.shape[1],))


def absorb(carried, queries, key_rows, value_rows):
    running_max, running_sum, weighted = carried
    scores = jnp.einsum(
        "sqhmd,snmd->shmqn", queries, key_rows, preferred_element_type=jnp.float32
    ) * HQK ** (-0.5)
    new_max = jnp.maximum(running_max, jnp.max(scores, axis=-1))
    rescale = jnp.exp(running_max - new_max)
    exponent = jnp.exp(scores - new_max[..., None])
    running_sum = running_sum * rescale + jnp.sum(exponent, axis=-1)
    weighted = weighted * rescale[..., None] + jnp.einsum(
        "shmqn,snv->shmqv",
        exponent.astype(jnp.bfloat16),
        value_rows,
        preferred_element_type=jnp.float32,
    )
    return (new_max, running_sum, weighted)


def absorb_blocks(carried, queries, key_rows, value_rows):
    row_count = key_rows.shape[1]
    block_size = math.gcd(row_count, 1024)

    def absorb_step(block_number, inner):
        first_row = block_number * block_size
        key_block = lax.dynamic_slice_in_dim(key_rows, first_row, block_size, 1)
        value_block = lax.dynamic_slice_in_dim(value_rows, first_row, block_size, 1)
        return absorb(inner, queries, key_block, value_block)

    return lax.fori_loop(0, row_count // block_size, absorb_step, carried)


def local(
    latents,
    condition,
    context,
    context_cond,
    shift_weight,
    scale_weight,
    out_gate_weight,
    pre_gain,
    post_gain,
    query_weight,
    key_weight,
    value_weight,
    head_gate_weight,
    lambdas,
    head_gain,
    out_weight,
):
    pair_width = 2 * HQK
    local_heads = query_weight.shape[1] // pair_width
    key_group = lax.axis_index("tp") * local_heads // (HEADS // KVH)
    silu_cond = jax.nn.silu(condition.astype(jnp.float32)).astype(jnp.bfloat16)
    silu_context = jax.nn.silu(context_cond.astype(jnp.float32)).astype(jnp.bfloat16)[None, :]
    shifts, scales, out_gate, context_shift, context_scale = (
        over_axes(
            jnp.dot(silu_cond, shift_weight, preferred_element_type=jnp.float32), ("sp", "tp")
        ),
        over_axes(
            jnp.dot(silu_cond, scale_weight, preferred_element_type=jnp.float32), ("sp", "tp")
        ),
        over_axes(
            jnp.dot(silu_cond, out_gate_weight, preferred_element_type=jnp.float32), ("sp", "tp")
        ),
        over_axes(
            jnp.dot(silu_context, shift_weight, preferred_element_type=jnp.float32), ("sp", "tp")
        ),
        over_axes(
            jnp.dot(silu_context, scale_weight, preferred_element_type=jnp.float32), ("sp", "tp")
        ),
    )
    latent_in = modulate(latents, pre_gain, shifts, scales)
    context_in = modulate(context, pre_gain, context_shift, context_scale)
    own_key_weight = lax.dynamic_slice_in_dim(key_weight, key_group * pair_width, pair_width, 1)
    own_value_weight = lax.dynamic_slice_in_dim(value_weight, key_group * HV, HV, 1)
    pieces = lax.all_gather(latent_in, "tp", axis=1, tiled=True)
    columns = [project(pieces, query_weight), project(pieces, head_gate_weight)]
    columns = columns + [project(pieces, own_key_weight), project(pieces, own_value_weight)]
    gathered = jnp.concatenate(columns, axis=-1)
    samples, row_count = (gathered.shape[0], gathered.shape[1])
    query_width = local_heads * pair_width
    gate_width = local_heads * HV
    queries = gathered[..., :query_width].reshape(samples, row_count, local_heads, 2, HQK)
    head_gate = gathered[..., query_width : query_width + gate_width]
    carried = (
        jnp.full((samples, local_heads, 2, row_count), -1e30, jnp.float32),
        jnp.zeros((samples, local_heads, 2, row_count), jnp.float32),
        jnp.zeros((samples, local_heads, 2, row_count, HV), jnp.float32),
    )
    context_keys = project(context_in, key_weight)
    context_values = project(context_in, value_weight)
    context_keys, context_values = in_one_piece((context_keys, context_values), ("sp", "tp"), 1, 0)
    key_part = lax.dynamic_slice_in_dim(context_keys, key_group * pair_width, pair_width, 2)
    key_part = key_part.reshape(key_part.shape[0], key_part.shape[1], 2, HQK)
    value_part = lax.dynamic_slice_in_dim(context_values, key_group * HV, HV, 2)
    key_part, value_part = (key_part, value_part)
    carried = absorb_blocks(carried, queries, key_part, value_part)
    own_keys = gathered[..., query_width + gate_width : query_width + gate_width + pair_width]
    own_values = gathered[..., query_width + gate_width + pair_width :]
    pieces = in_one_piece((own_keys, own_values), "sp", 1, 0)
    key_part = pieces[0].reshape(pieces[0].shape[0], pieces[0].shape[1], 2, HQK)
    carried = absorb_blocks(carried, queries, key_part, pieces[1])
    running_max, running_sum, weighted = carried
    ratios = weighted / running_sum[..., None]
    attended = ratios[:, :, 0] - lambdas[None, :, None, None] * ratios[:, :, 1]
    attended = jnp.transpose(attended, (0, 2, 1, 3))
    gate_input = head_gate.reshape(samples, row_count, local_heads, HV).astype(jnp.float32)
    branch = (norm_rows(attended, head_gain) * jax.nn.silu(gate_input)).astype(jnp.bfloat16)
    branch = branch.reshape(samples, row_count, gate_width)
    projected = jnp.einsum(
        "sqc,cd->sqd",
        gathered_copies(branch, "tp", 2),
        out_weight,
        preferred_element_type=jnp.float32,
    )
    projected = lax.all_to_all(
        projected.astype(jnp.bfloat16), "tp", split_axis=1, concat_axis=2, tiled=True
    )
    mixed_out = out_gate[:, None, :] * norm_rows(projected.astype(jnp.float32), post_gain)
    return mixed_out.astype(jnp.bfloat16)


def solution(mesh):
    return jax.shard_map(
        local,
        mesh=mesh,
        in_specs=(
            P("dp", ("sp", "tp"), None),
            P("dp", ("sp", "tp")),
            P("dp", ("sp", "tp"), None),
            P(("sp", "tp")),
            P(("sp", "tp"), None),
            P(("sp", "tp"), None),
            P(("sp", "tp"), None),
            P(),
            P(),
            P(None, "tp"),
            P(),
            P(),
            P(None, "tp"),
            P("tp"),
            P(),
            P(None, "tp"),
        ),
        out_specs=P("dp", ("sp", "tp"), None),
        check_vma=False,
    )
```

profile of v0, /device:TPU:2, one launch (start us, length us, event | category | flops | bytes accessed | tf_op | source)
XLA Modules:
  0.0 325.7 jit_solution(14912803270171013887)
XLA Ops:
  6.5 1.2 fusion.92
  7.8 1.1 fusion.94
  8.9 1.1 fusion.96
  10.0 1.1 fusion.98
  11.1 1.1 fusion.100
  12.2 53.1 %all-reduce = (f32[1,3072]{1,0:T(1,128)S(1)}, f32[1,3072]{1,0:T(1,128)S(1)}, f32[1,3072]{1,0:T(1,128)S(1)}, f32[1,3072]{1,0:T(1,128)S(1)}, f32[1,3072]{1,0:T(1,128)S(1)}) all-reduce(f32[1,3072]{1,0:T(1,128)S(1)} %fusion.96, f32[1,3072]{1,0:T(1,128)S(1)} %fusion.98, ...), channel_id=1, replica_groups=mesh['sp'=12,'tp'=8,'dp'=8] {'sp'}, use_global_device_ids=true, to_apply=%region_10.11 | all-reduce | flops 15360 | bytes 122880 | tf_op jit(solution)/shard_map/psum | solution.py:19
  65.3 30.9 %all-reduce.1 = (f32[3072]{0:T(1024)S(1)}, f32[1,3072]{1,0:T(1,128)S(1)}, f32[3072]{0:T(1024)S(1)}, f32[1,3072]{1,0:T(1,128)S(1)}, f32[3072]{0:T(1024)}) all-reduce(f32[3072]{0:T(1024)S(1)} %bitcast.243, f32[1,3072]{1,0:T(1,128)S(1)} %get-tuple-element.335, f32[3072]{0:T(1024)S(1)} %bitcast.244, ...), channel_id=1, replica_groups=mesh['sp'=12,'tp'=8,'dp'=8] {'tp'}, use_global_device_ids=true, to_apply=%region_11.12 | all-reduce | flops 15360 | bytes 122880 | tf_op jit(solution)/shard_map/psum | solution.py:19
  96.2 1.2 fusion.71
  97.4 2.0 fusion.75
  99.5 43.6 %all-gather.3.cloned.1.call-done = bf16[1,512,3072]{2,1,0:T(8,128)(2,1)} async-done(((bf16[1,64,3072]{2,1,0:T(8,128)(2,1)}), bf16[1,512,3072]{2,1,0:T(8,128)(2,1)}) %all-gather.3.cloned.1.call-update) | async-done | bytes 3145744 | tf_op jit(solution)/shard_map/all_gather | solution.py:140
  143.1 3.2 fusion.63
  146.3 1.0 fusion.66
  147.3 0.7 pad_maximum_fusion
  148.7 1.8 fusion.70
  150.5 71.0 %all_gather.9 = bf16[2,384,256]{2,0,1:T(2,128)(2,1)S(1)} all-gather(bf16[2,4,256]{2,0,1:T(2,128)(2,1)S(1)} %copy.39), channel_id=1, replica_groups=mesh['sp'=12,'tp'=8,'dp'=8] {'sp','tp'}, dimensions={1}, use_global_device_ids=true | all-gather | bytes 397312 | tf_op jit(solution)/shard_map/all_gather | solution.py:26
  222.2 0.8 copy.50
  224.5 3.1 fusion.48
  227.6 7.2 %while.36 = (s32[]{:T(128)}, f32[1,1,2,512]{3,2,1,0:T(2,128)S(1)}, f32[1,1,2,512]{3,2,1,0:T(2,128)S(1)}, f32[1,1,2,512,128]{4,3,2,1,0:T(8,128)S(1)}, bf16[1,384,...) while((s32[]{:T(128)}, f32[1,1,2,512]{3,2,1,0:T(2,128)S(1)}, ...), condition=%wide.region_15.16_spmd.clone, body=%wide.region_12.15_spmd.clone.sunk | while | flops 51517448 | bytes 2883759 | solution.py:93
  227.6 1.0 fusion.141
  228.7 1.2 fusion.144
  230.0 1.0 fusion.141
  231.1 1.2 fusion.144
  232.4 1.0 fusion.141
  233.5 1.2 fusion.144
  234.8 3.8 %fusion.110 = (bf16[1,6144,128]{2,1,0:T(8,128)(2,1)}, bf16[1,6144,128]{2,1,0:T(8,128)(2,1)}) fusion(bf16[2,6144,128]{2,1,0:T(8,128)(2,1)} %all-gather.5.cloned.1.call-done), kind=kLoop, calls=%fused_computation.125 | loop fusion | bytes 6291456 | tf_op jit(solution)/shard_map/split | solution.py:27
  238.6 2.6 copy.42
  241.2 26.7 %while.35 = (s32[]{:T(128)}, f32[1,1,2,512]{3,2,1,0:T(2,128)S(1)}, f32[1,1,2,512]{3,2,1,0:T(2,128)S(1)}, f32[1,1,2,512,128]{4,3,2,1,0:T(8,128)S(1)}, bf16[1,6144...) while((s32[]{:T(128)}, f32[1,1,2,512]{3,2,1,0:T(2,128)S(1)}, ...), condition=%wide.region_19.20_spmd, body=%wide.region_16.19_spmd.sunk | while | flops 411307008 | bytes 14352547 | solution.py:93
  241.2 1.8 bitcast_reduce_fusion.2
  243.0 1.9 fusion.138
  244.9 0.7 fusion.137
  245.7 1.7 bitcast_reduce_fusion.2
  247.4 1.9 fusion.138
  250.1 1.7 bitcast_reduce_fusion.2
  251.9 1.9 fusion.138
  254.6 1.7 bitcast_reduce_fusion.2
  256.3 1.9 fusion.138
  259.0 1.7 bitcast_reduce_fusion.2
  260.7 1.9 fusion.138
  263.4 1.7 bitcast_reduce_fusion.2
  265.2 1.9 fusion.138
  268.3 2.9 fusion.81
  271.4 23.6 %all_to_all.14 = bf16[8,1,512,128]{2,3,1,0:T(8,128)(2,1)S(1)} all-to-all(bf16[8,1,512,128]{2,3,1,0:T(8,128)(2,1)S(1)} %broadcast_in_dim.23), channel_id=1, replica_groups=mesh['sp'=12,'tp'=8,'dp'=8] {'tp'}, dimensions={0} | all-to-all | bytes 2097152 | tf_op jit(solution)/shard_map/all_to_all | solution.py:32
  295.0 0.7 fusion.47
  296.9 3.0 reduce.22
  300.0 14.3 %all_to_all.15 = bf16[8,2,12288]{2,1,0:T(2,128)(2,1)S(1)} all-to-all(bf16[8,2,12288]{2,1,0:T(2,128)(2,1)S(1)} %reshape.424), channel_id=1, replica_groups=mesh['sp'=12,'tp'=8,'dp'=8] {'tp'}, dimensions={0} | all-to-all | bytes 786432 | tf_op jit(solution)/shard_map/all_to_all | solution.py:180
  314.7 0.8 bitcast_convert_fusion
  315.5 1.7 multiply_reduce_fusion
  317.9 0.9 multiply_convert_fusion
  (89 shorter events, 9.2 us)
Async XLA Ops:
  6.5 139.8 %copy-start = (bf16[3072,256]{1,0:T(8,128)(2,1)S(1)}, bf16[3072,256]{1,0:T(8,128)(2,1)}, u32[]{:S(2)}) copy-start(bf16[3072,256]{1,0:T(8,128)(2,1)} %param.30) | copy-start | bytes 4718596
  6.5 136.5 %all-gather.3.cloned.1.call-start = ((), (), s32[]{:S(2)}) async-start(), calls=%async_computation.2 | async-start | bytes 3538944 | tf_op jit(solution)/shard_map/all_gather | solution.py:140
  99.4 135.4 %all-gather.5.cloned.1.call-start = ((), (), s32[]{:S(2)}) async-start(), calls=%async_computation.3 | async-start | bytes 3407872 | tf_op jit(solution)/shard_map/all_gather | solution.py:26
  143.1 3.2 copy-start.1
  146.3 1.8 copy-start.3
  146.3 2.0 copy-start.4
  148.3 76.2 %copy-start.2 = (bf16[3072,128]{1,0:T(8,128)(2,1)S(1)}, bf16[3072,128]{1,0:T(8,128)(2,1)}, u32[]{:S(2)}) copy-start(bf16[3072,128]{1,0:T(8,128)(2,1)} %param.29) | copy-start | bytes 2359300
  241.2 27.1 %copy-start.7 = (bf16[3072,128]{1,0:T(8,128)(2,1)S(1)}, bf16[3072,128]{1,0:T(8,128)(2,1)}, u32[]{:S(2)}) copy-start(bf16[3072,128]{1,0:T(8,128)(2,1)} %param.32) | copy-start | bytes 2359300
  241.2 27.1 %copy-start.9 = (f32[128]{0:T(128)S(1)}, f32[128]{0:T(128)}, u32[]{:S(2)}) copy-start(f32[128]{0:T(128)} %param.34) | copy-start | bytes 1540
  271.2 23.9 %copy-start.8 = (bf16[1024,384]{1,0:T(8,128)(2,1)S(1)}, bf16[1024,384]{1,0:T(8,128)(2,1)}, u32[]{:S(2)}) copy-start(bf16[1024,384]{1,0:T(8,128)(2,1)} %param.35) | copy-start | bytes 2359300
  314.3 3.6 %copy-start.5 = (f32[3072]{0:T(1024)S(1)}, f32[3072]{0:T(1024)}, u32[]{:S(2)}) copy-start(f32[3072]{0:T(1024)} %param.28) | copy-start | bytes 36868
  314.3 3.6 %copy-start.6 = (f32[3072]{0:T(1024)S(1)}, f32[3072]{0:T(1024)}, u32[]{:S(2)}) copy-start(f32[3072]{0:T(1024)} %get-tuple-element.343) | copy-start | bytes 36868
Sparse Core Ops, SparseCore 0:
  99.5 43.4 all-gather.2
  148.2 63.0 all-gather.4
where the time goes:
time: 327 us; the launch traced here: 326 us
  blocking collectives  193 us (59%)
  matrix products  47.2 us (14%)
  waiting for transfers between devices  43.6 us (13%)
  other arithmetic  15.7 us (5%)
  between operations  14.4 us (4%)
  local copies, waits for them, and re-layouts  11.3 us (3%)
    psum x2, blocking collectives, over_axes(): shard = lax.psum(shard, axis)  84.1 us
    all_gather x1, blocking collectives, in_one_piece(): whole = lax.all_gather(both, axis, axis=dim, tiled=True)  71 us
    all_gather x1, waiting for transfers between devices, local(): pieces = lax.all_gather(latent_in, 'tp', axis=1, tiled=True)  43.6 us
    all_to_all x1, blocking collectives, copy_for_each(): return lax.all_to_all(copies, axis, split_axis=0, concat_axis=0, tiled=True)  23.6 us
    dot_general x9, matrix products, absorb(): jnp.einsum('shmqn,snv->shmqv', exponent.astype(jnp.bfloat16), value_rows,...  15.1 us
    all_to_all x1, blocking collectives, local(): lax.all_to_all(projected.astype(jnp.bfloat16), 'tp', split_axis=1, concat...  14.3 us
    dot_general x9, matrix products, absorb(): jnp.einsum('sqhmd,snmd->shmqn', queries, key_rows, preferred_element_type...  13.5 us
    dot_general x6, matrix products, project(): jnp.dot(flattened, weight, preferred_element_type=jnp.float32)  12.3 us
  transfers between devices with their start and end apart: 2, of which 1 were waited for; matrix products, arithmetic and copies ran while one was open for 5% of the time, Pallas kernels for 0%

commit v1 on v0

v1 whole, which is shorter than its diff:
```python
import jax
import jax.numpy as jnp
from jax import lax
from jax.experimental import pallas as pl
from jax.experimental.pallas import tpu as pltpu
from jax.sharding import PartitionSpec as P

D = 3072
GROUP = 4
HQK = 64
HV = 128
ROWS = 64
CTX_ROWS = 4
TP = 8
SP = 12
QUARTER = 2 * (ROWS + CTX_ROWS)
KEYS = SP * QUARTER
MESSAGE = GROUP * 2 * HV + 2 * HV
CHUNK = 256
VECTOR_ROWS = D // CHUNK
SCALE = HQK ** (-0.5) * 1.4426950408889634
NORM_EPSILON = 1e-06
F32 = jnp.float32
BF16 = jnp.bfloat16
TP_GROUPS = [[0, 1, 2, 3], [4, 5, 6, 7]]
VMEM_LIMIT = 60 * 1024 * 1024


def silu(values):
    return values / (1.0 + jnp.exp(-values))


def partial_sums_kernel(cond_ref, ctx_ref, shift_ref, scale_ref, gate_ref, out_ref):
    both = jnp.concatenate([cond_ref[...], ctx_ref[...]], axis=0).astype(F32)
    both = silu(both).astype(BF16)
    out_ref[...] = jnp.zeros_like(out_ref)
    shift = jnp.dot(both, shift_ref[...], preferred_element_type=F32)
    scale = jnp.dot(both, scale_ref[...], preferred_element_type=F32)
    gate = jnp.dot(both, gate_ref[...], preferred_element_type=F32)
    vectors = [shift[:1], scale[:1], gate[:1], shift[1:], scale[1:]]
    for number, vector in enumerate(vectors):
        for piece in range(VECTOR_ROWS):
            row = number * VECTOR_ROWS + piece
            out_ref[row : row + 1, :] = vector[:, piece * CHUNK : (piece + 1) * CHUNK]


def vector_of(sums_ref, number):
    first = number * VECTOR_ROWS
    return jnp.concatenate(
        [sums_ref[first + piece : first + piece + 1, :] for piece in range(VECTOR_ROWS)], axis=1
    )


def project_kernel(
    quarter_ref, rows_ref, sums_ref, gain_ref, qg_weight_ref, kv_weight_ref,
    q_ref, gate_ref, kv_ref, latent_ref, context_ref,
):
    step = pl.program_id(0)
    gain = gain_ref[...]
    values = rows_ref[0].astype(F32)
    normed = values * lax.rsqrt(jnp.mean(values * values, axis=-1, keepdims=True) + NORM_EPSILON)
    latent = normed[:ROWS] * (gain * (1.0 + vector_of(sums_ref, 1))) + vector_of(sums_ref, 0)
    context = normed[ROWS:] * (gain * (1.0 + vector_of(sums_ref, 4))) + vector_of(sums_ref, 3)
    latent_ref[pl.ds(pl.multiple_of(step * ROWS, ROWS), ROWS), :] = latent.astype(BF16)
    context_ref[step, :CTX_ROWS, :] = context

    @pl.when(step == TP - 1)
    def _():
        projected = jnp.dot(latent_ref[...], qg_weight_ref[...], preferred_element_type=F32)
        q_ref[...] = projected[:, :HV].astype(BF16)
        gate_ref[...] = projected[:, HV:].astype(BF16)
        quarter = quarter_ref[0]
        first = pl.multiple_of(quarter * 2 * ROWS, 2 * ROWS)
        kv = jnp.dot(
            latent_ref[pl.ds(first, 2 * ROWS), :], kv_weight_ref[...], preferred_element_type=F32
        )
        kv_ref[: 2 * ROWS, :] = kv.astype(BF16)
        own_context = jnp.concatenate(
            [context_ref[2 * quarter, :CTX_ROWS, :], context_ref[2 * quarter + 1, :CTX_ROWS, :]],
            axis=0,
        ).astype(BF16)
        kv = jnp.dot(own_context, kv_weight_ref[...], preferred_element_type=F32)
        kv_ref[2 * ROWS :, :] = kv.astype(BF16)


def three_parts(value):
    high = value.astype(BF16)
    rest = value - high.astype(F32)
    middle = rest.astype(BF16)
    low = (rest - middle.astype(F32)).astype(BF16)
    return high.astype(F32), middle.astype(F32), low.astype(F32)


def attention_kernel(lambda_ref, q_ref, kv_ref, gate_ref, out_ref):
    peers = out_ref.shape[0]
    block = peers * ROWS
    q = q_ref[...].reshape(GROUP * block, 2 * HQK)
    keys = kv_ref[:, : 2 * HQK]
    value_rows = kv_ref[:, 2 * HQK :]
    lane = lax.broadcasted_iota(jnp.int32, q.shape, 1)
    stat_lane = lax.broadcasted_iota(jnp.int32, (block, HV), 1)
    stats = jnp.zeros((block, HV), F32)
    for part, piece in enumerate(three_parts(jnp.full((block, HV), lambda_ref[0], F32))):
        stats = jnp.where(stat_lane == part * 32 + 2 * GROUP, piece, stats)
    for m in range(2):
        one_map = jnp.where(lane // HQK == m, q, jnp.zeros_like(q))
        scores = lax.dot_general(
            one_map, keys, (((1,), (1,)), ((), ())), preferred_element_type=F32
        )
        largest = jnp.max(scores, axis=-1, keepdims=True) * SCALE
        exponent = jnp.exp2(scores * SCALE - largest)
        total = jnp.sum(exponent, axis=-1, keepdims=True)
        weighted = jnp.dot(exponent.astype(BF16), value_rows, preferred_element_type=F32)
        ratio = (weighted / total).astype(BF16)
        level = largest + jnp.log2(total)
        for h in range(GROUP):
            column = (2 * h + m) * HV
            for p in range(peers):
                first = h * block + p * ROWS
                out_ref[p, :, column : column + HV] = ratio[first : first + ROWS]
            wide = jnp.broadcast_to(level[h * block : (h + 1) * block], (block, HV))
            for part, piece in enumerate(three_parts(wide)):
                stats = jnp.where(stat_lane == part * 32 + 2 * h + m, piece, stats)
    for p in range(peers):
        out_ref[p, :, 2 * GROUP * HV : 2 * GROUP * HV + HV] = gate_ref[p * ROWS : (p + 1) * ROWS, :]
        out_ref[p, :, 2 * GROUP * HV + HV :] = stats[p * ROWS : (p + 1) * ROWS].astype(BF16)


def finish_kernel(
    parts_ref, weight_ref, sums_ref, post_gain_ref, head_gain_ref, out_ref, branch_ref, projected_ref
):
    step = pl.program_id(0)

    @pl.when(step == 0)
    def _():
        gate_column = 2 * GROUP * HV
        levels = []
        for t in range(TP):
            stats = parts_ref[t, :, gate_column + HV :].astype(F32)
            levels.append(stats[:, :32] + stats[:, 32:64] + stats[:, 64:96])
        for g in range(TP // GROUP):
            members = range(g * GROUP, (g + 1) * GROUP)
            top = levels[members[0]]
            for t in members[1:]:
                top = jnp.maximum(top, levels[t])
            shares = [jnp.exp2(levels[t] - top) for t in members]
            total = shares[0] + shares[1] + shares[2] + shares[3]
            shares = [share / total for share in shares]
            for j in range(GROUP):
                head = g * GROUP + j
                ratios = []
                for m in range(2):
                    index = 2 * j + m
                    ratio = jnp.zeros((ROWS, HV), F32)
                    for t, share in zip(members, shares):
                        part = parts_ref[t, :, index * HV : (index + 1) * HV].astype(F32)
                        ratio = ratio + share[:, index : index + 1] * part
                    ratios.append(ratio)
                own_lambda = levels[head][:, 2 * GROUP : 2 * GROUP + 1]
                attended = ratios[0] - own_lambda * ratios[1]
                square = jnp.mean(attended * attended, axis=-1, keepdims=True)
                gate = parts_ref[head, :, gate_column : gate_column + HV].astype(F32)
                branch = attended * lax.rsqrt(square + NORM_EPSILON) * head_gain_ref[...] * silu(gate)
                branch_ref[:, head * HV : (head + 1) * HV] = branch.astype(BF16)

    projected = jnp.dot(branch_ref[...], weight_ref[0], preferred_element_type=F32)
    projected_ref[step] = projected.astype(BF16).astype(F32)

    @pl.when(step == TP - 1)
    def _():
        square = jnp.zeros((ROWS, 1), F32)
        for t in range(TP):
            square = square + jnp.sum(projected_ref[t] * projected_ref[t], axis=-1, keepdims=True)
        factor = lax.rsqrt(square / D + NORM_EPSILON)
        out_gate = vector_of(sums_ref, 2)
        gain = post_gain_ref[...]
        width = D // TP
        for t in range(TP):
            columns = slice(t * width, (t + 1) * width)
            value = projected_ref[t] * factor * gain[:, columns] * out_gate[:, columns]
            out_ref[:, columns] = value.astype(BF16)


def summed(partials):
    axes = ("sp", "tp")
    pieces = lax.all_to_all(partials, axes, split_axis=0, concat_axis=0, tiled=True)
    own = jnp.sum(pieces, axis=0, keepdims=True)
    copies = jnp.broadcast_to(own, pieces.shape)
    return lax.all_to_all(copies, axes, split_axis=0, concat_axis=0, tiled=True)


def whole_block(shape):
    return pl.BlockSpec(shape, lambda *_: (0,) * len(shape))


def local(
    latents, condition, context, context_cond, shift_weight, scale_weight, out_gate_weight,
    pre_gain, post_gain, query_weight, key_weight, value_weight, head_gate_weight,
    lambdas, head_gain, out_weight,
):
    params = pltpu.CompilerParams(vmem_limit_bytes=VMEM_LIMIT)
    t = lax.axis_index("tp")
    key_group, quarter = t // GROUP, t % GROUP
    with jax.named_scope("gather_rows"):
        rows = jnp.concatenate([latents[0], context[0]], axis=0)
        rows = lax.all_gather(rows, "tp", axis=0, tiled=False)
    with jax.named_scope("modulation"):
        partials = pl.pallas_call(
            partial_sums_kernel,
            out_shape=jax.ShapeDtypeStruct((SP * TP, CHUNK), F32),
            compiler_params=params,
            name="partial_sums",
        )(condition, context_cond[None, :], shift_weight, scale_weight, out_gate_weight)
        sums = summed(partials)
    with jax.named_scope("gather_out_weight"):
        after = out_weight + rows[0, 0, 0] * jnp.zeros((), BF16)
        out_weights = lax.all_gather(after, "tp", axis=0, tiled=False)
    qg_weight = jnp.concatenate([query_weight, head_gate_weight], axis=1)
    kv_weight = jnp.concatenate(
        [
            lax.dynamic_slice_in_dim(key_weight, key_group * 2 * HQK, 2 * HQK, 1),
            lax.dynamic_slice_in_dim(value_weight, key_group * HV, HV, 1),
        ],
        axis=1,
    )
    per_device = ROWS + CTX_ROWS
    with jax.named_scope("project"):
        queries, head_gate, key_values = pl.pallas_call(
            project_kernel,
            grid_spec=pltpu.PrefetchScalarGridSpec(
                num_scalar_prefetch=1,
                grid=(TP,),
                in_specs=[
                    pl.BlockSpec((1, per_device, D), lambda i, _: (i, 0, 0)),
                    whole_block((SP * TP, CHUNK)),
                    whole_block((1, D)),
                    whole_block((D, 2 * HV)),
                    whole_block((D, 2 * HV)),
                ],
                out_specs=[
                    whole_block((TP * ROWS, HV)),
                    whole_block((TP * ROWS, HV)),
                    whole_block((QUARTER, 2 * HV)),
                ],
                scratch_shapes=[
                    pltpu.VMEM((TP * ROWS, D), BF16),
                    pltpu.VMEM((TP, 2 * CTX_ROWS, D), F32),
                ],
            ),
            out_shape=[
                jax.ShapeDtypeStruct((TP * ROWS, HV), BF16),
                jax.ShapeDtypeStruct((TP * ROWS, HV), BF16),
                jax.ShapeDtypeStruct((QUARTER, 2 * HV), BF16),
            ],
            compiler_params=params,
            name="project",
        )(quarter.astype(jnp.int32)[None], rows, sums, pre_gain[None, :], qg_weight, kv_weight)
    with jax.named_scope("gather_keys"):
        key_values = lax.all_gather(key_values, "sp", axis=0, tiled=True)
    with jax.named_scope("exchange_queries"):
        copies = jnp.broadcast_to(queries[None], (GROUP, TP * ROWS, HV))
        copies = lax.all_to_all(
            copies, "tp", split_axis=0, concat_axis=0, axis_index_groups=TP_GROUPS, tiled=True
        )
    peers = 2
    with jax.named_scope("attention"):
        parts = pl.pallas_call(
            attention_kernel,
            grid=(TP // peers,),
            in_specs=[
                pl.BlockSpec(memory_space=pltpu.SMEM),
                pl.BlockSpec((GROUP, peers * ROWS, HV), lambda i: (0, i, 0)),
                whole_block((KEYS, 2 * HV)),
                pl.BlockSpec((peers * ROWS, HV), lambda i: (i, 0)),
            ],
            out_specs=pl.BlockSpec((peers, ROWS, MESSAGE), lambda i: (i, 0, 0)),
            out_shape=jax.ShapeDtypeStruct((TP, ROWS, MESSAGE), BF16),
            compiler_params=params,
            name="attention",
        )(lambdas, copies, key_values, head_gate)
    with jax.named_scope("exchange_parts"):
        parts = lax.all_to_all(parts, "tp", split_axis=0, concat_axis=0, tiled=True)
    with jax.named_scope("finish"):
        mixed_out = pl.pallas_call(
            finish_kernel,
            grid=(TP,),
            in_specs=[
                whole_block((TP, ROWS, MESSAGE)),
                pl.BlockSpec((1, GROUP * 2 * HV, D // TP), lambda i: (i, 0, 0)),
                whole_block((SP * TP, CHUNK)),
                whole_block((1, D)),
                whole_block((1, HV)),
            ],
            out_specs=whole_block((ROWS, D)),
            out_shape=jax.ShapeDtypeStruct((ROWS, D), BF16),
            scratch_shapes=[
                pltpu.VMEM((ROWS, GROUP * 2 * HV), BF16),
                pltpu.VMEM((TP, ROWS, D // TP), F32),
            ],
            compiler_params=params,
            name="finish",
        )(parts, out_weights, sums, post_gain[None, :], head_gain[None, :])
    return mixed_out[None]


def solution(mesh):
    tokens = P("dp", ("sp", "tp"), None)
    channels = P(("sp", "tp"), None)
    return jax.shard_map(
        local,
        mesh=mesh,
        in_specs=(
            tokens, P("dp", ("sp", "tp")), tokens, P(("sp", "tp")), channels, channels, channels,
            P(), P(), P(None, "tp"), P(), P(), P(None, "tp"), P("tp"), P(), P(None, "tp"),
        ),
        out_specs=tokens,
        check_vma=False,
    )
```

time: 327 us -> 236 us (0.72)
  blocking collectives: 193 us -> 59.3 us
  matrix products: 47.2 us -> 0 us
  waiting for transfers between devices: 43.6 us -> 88.2 us
  Pallas kernels: 0 us -> 36.9 us
  starting transfers between devices: 0.04 us -> 23.8 us
  other arithmetic: 15.7 us -> 5.7 us
  local copies, waits for them, and re-layouts: 11.3 us -> 6.93 us
    psum x2 -> x0, blocking collectives: 84.1 us -> none  [over_axes(): shard = lax.psum(shard, axis)]
    dot_general x30 -> x0, matrix products: 47.2 us -> none  [the longest x9 15.1 us: absorb(): jnp.einsum('shmqn,snv->shmqv', exponent.astype(jnp.bfloat16), value_rows,...]
    all_gather x1, blocking collectives: 71 us -> 28.2 us  [local(): key_values = lax.all_gather(key_values, 'sp', axis=0, tiled=True)]
    pallas_call x0 -> x4, Pallas kernels: none -> 36.9 us  [the longest x1 16.8 us: local(): pl.pallas_call(attention_kernel, grid=(TP // peers,), in_specs=[pl.BlockS...]
    all_to_all x0 -> x3, waiting for transfers between devices: none -> 26.5 us  [the longest x1 13.3 us: summed(): lax.all_to_all(partials, axes, split_axis=0, concat_axis=0, tiled=True)]
    all_to_all x0 -> x3, starting transfers between devices: none -> 23.8 us  [the longest x1 14.4 us: summed(): lax.all_to_all(partials, axes, split_axis=0, concat_axis=0, tiled=True)]
    all_gather x2, waiting for transfers between devices: 43.6 us -> 61.6 us  [the longest x1 61.6 us: local(): rows = lax.all_gather(rows, 'tp', axis=0, tiled=False)]
    reduce_sum x14 -> x1, other arithmetic: 7.69 us -> 0.12 us  [summed(): own = jnp.sum(pieces, axis=0, keepdims=True)]
  transfers between devices with their start and end apart: 2 -> 5, of which waited for: 1 -> 3; matrix products, arithmetic and copies ran while one was open for 5% -> 3% of each run, Pallas kernels for 0% -> 12%
where the time goes in v1:
time: 236 us
  waiting for transfers between devices  88.2 us (37%)
  blocking collectives  59.3 us (25%)
  Pallas kernels  36.9 us (16%)
  starting transfers between devices  23.8 us (10%)
  between operations  14.8 us (6%)
  local copies, waits for them, and re-layouts  6.93 us (3%)
  other arithmetic  5.7 us (2%)
    all_gather x1, waiting for transfers between devices, local(): rows = lax.all_gather(rows, 'tp', axis=0, tiled=False)  61.6 us
    all_to_all x1, blocking collectives, local(): parts = lax.all_to_all(parts, 'tp', split_axis=0, concat_axis=0, tiled=True)  31.1 us
    all_gather x1, blocking collectives, local(): key_values = lax.all_gather(key_values, 'sp', axis=0, tiled=True)  28.2 us
    pallas_call x1, Pallas kernels, local(): pl.pallas_call(attention_kernel, grid=(TP // peers,), in_specs=[pl.BlockS...  16.8 us
    all_to_all x1, starting transfers between devices, summed(): lax.all_to_all(partials, axes, split_axis=0, concat_axis=0, tiled=True)  14.4 us
    all_to_all x1, waiting for transfers between devices, summed(): lax.all_to_all(partials, axes, split_axis=0, concat_axis=0, tiled=True)  13.3 us
    all_to_all x1, waiting for transfers between devices, summed(): return lax.all_to_all(copies, axes, split_axis=0, concat_axis=0, tiled=True)  13.3 us
    pallas_call x1, Pallas kernels, local(): pl.pallas_call(project_kernel, grid_spec=pltpu.PrefetchScalarGridSpec(num...  9.03 us
  transfers between devices with their start and end apart: 5, of which 3 were waited for; matrix products, arithmetic and copies ran while one was open for 3% of the time, Pallas kernels for 12%

profile of v1, /device:TPU:2, one launch (start us, length us, event | category | flops | bytes accessed | tf_op | source)
XLA Modules:
  0.0 235.7 jit_solution(7896678777865492382)
XLA Ops:
  6.5 0.0 copy-start.1
  6.5 0.0 all-gather.8.cloned.1.call-start
  6.5 1.9 maximum_bitcast_fusion
  8.4 0.0 all-gather.8.cloned.1.call-update
  8.5 0.0 all-gather.6.cloned.1.call-start
  8.5 61.6 %all-gather.8.cloned.1.call-done.rows_ref = bf16[8,68,3072]{2,1,0:T(8,128)(2,1)} async-done(((bf16[1,68,3072]{2,1,0:T(8,128)(2,1)}), bf16[8,68,3072]{2,1,0:T(8,128)(2,1)}) %all-gather.8.cloned.1.call-update) | async-done | bytes 3342352 | tf_op jit(solution)/shard_map/gather_rows/all_gather | solution.py:206
  70.1 1.1 slice.4
  71.9 0.0 copy-done.1
  71.9 0.0 copy-start.4
  71.9 1.0 broadcast_add_fusion
  72.9 0.0 copy-start.5
  72.9 0.0 all-gather.6.cloned.1.call-update
  72.9 2.1 partial_sums.1
  75.1 1.6 copy.17
  76.7 14.4 %all-to-all-start = ((f32[96,1,256]{2,1,0:T(1,128)}), f32[96,1,256]{2,1,0:T(1,128)S(1)}, u32[]{:S(2)}, u32[]{:S(2)}) async-start(f32[96,1,256]{2,1,0:T(1,128)} %copy.17), calls=%async_computation | async-start | bytes 196608 | tf_op jit(solution)/shard_map/modulation/all_to_all | solution.py:186
  91.1 0.0 copy-done.4
  91.1 0.0 copy-done.5
  91.2 0.1 constant_dynamic-slice_fusion
  91.3 0.0 copy-start.2
  91.3 0.0 copy-start.3
  91.3 1.3 pad_maximum_fusion.1.kv_weight_ref
  92.6 13.3 %all-to-all-done = f32[96,1,256]{2,1,0:T(1,128)S(1)} async-done(((f32[96,1,256]{2,1,0:T(1,128)}), f32[96,1,256]{2,1,0:T(1,128)S(1)}, u32[]{:S(2)}, u32[]{:S(2)}) %all-to-all-start) | async-done | bytes 98336 | tf_op jit(solution)/shard_map/modulation/all_to_all | solution.py:186
  105.9 0.1 reduce_sum.9
  106.0 0.7 broadcast_in_dim.32
  106.7 5.9 %all-to-all-start.1 = ((f32[96,1,256]{2,1,0:T(1,128)}), f32[96,1,256]{2,1,0:T(1,128)S(1)}, u32[]{:S(2)}, u32[]{:S(2)}) async-start(f32[96,1,256]{2,1,0:T(1,128)} %broadcast_in_dim.32), calls=%async_computation.1 | async-start | bytes 196608 | tf_op jit(solution)/shard_map/modulation/all_to_all | solution.py:189
  112.7 0.0 copy-done.2
  112.7 0.0 copy-done.3
  112.7 1.4 pad_maximum_fusion.qg_weight_ref
  114.1 13.3 %all-to-all-done.1 = f32[96,1,256]{2,1,0:T(1,128)S(1)} async-done(((f32[96,1,256]{2,1,0:T(1,128)}), f32[96,1,256]{2,1,0:T(1,128)S(1)}, u32[]{:S(2)}, u32[]{:S(2)}) %all-to-all-start.1) | async-done | bytes 98336 | tf_op jit(solution)/shard_map/modulation/all_to_all | solution.py:189
  127.3 0.7 copy.20
  128.0 9.0 %project.1 = (bf16[512,128]{1,0:T(8,128)(2,1)}, bf16[512,128]{1,0:T(8,128)(2,1)}, bf16[136,256]{1,0:T(8,128)(2,1)}) custom-call(s32[1]{0:T(128)} %bitcast.quarter_ref, bf16[8,68,3072]{2,1,0:T(8,128)(2,1)} %all-gather.8.cloned.1.call-done.rows_ref, f32[96,256]{1,0:T(8,128)} %bitcast.17, f32[1,3072]{1,0:T(1,128)} %bitcast.22, ...), custom_call_target="tpu_custom_call" | custom-call | tf_op jit(solution)/shard_map/project/project/pallas_call | solution.py:228
  137.0 0.0 copy-start.6
  137.0 1.8 broadcast_in_dim.34
  138.8 3.5 %all-to-all-start.2 = ((bf16[4,512,128]{2,1,0:T(8,128)(2,1)}), bf16[4,512,128]{2,1,0:T(8,128)(2,1)S(1)}, u32[]{:S(2)}, u32[]{:S(2)}) async-start(bf16[4,512,128]{2,1,0:T(8,128)(2,1)} %broadcast_in_dim.34), calls=%async_computation.2 | async-start | bytes 1048576 | tf_op jit(solution)/shard_map/exchange_queries/all_to_all | solution.py:262
  143.0 0.0 copy-done.6
  143.0 28.2 %all_gather.17.kv_ref = bf16[1632,256]{1,0:T(8,128)(2,1)} all-gather(bf16[136,256]{1,0:T(8,128)(2,1)S(1)} %copy-done.6), channel_id=1, replica_groups=mesh['sp'=12,'tp'=8,'dp'=8] {'sp'}, dimensions={0}, use_global_device_ids=true | all-gather | bytes 905216 | tf_op jit(solution)/shard_map/gather_keys/all_gather | solution.py:259
  171.1 0.0 all-to-all-done.2.q_ref
  171.1 0.0 copy-start
  171.1 0.9 copy-done
  172.0 16.8 %attention.1 = bf16[8,64,1280]{2,1,0:T(8,128)(2,1)} custom-call(f32[1]{0:T(128)S(6)} %copy.21.lambda_ref, bf16[4,512,128]{2,1,0:T(8,128)(2,1)} %copy-done, bf16[1632,256]{1,0:T(8,128)(2,1)} %all_gather.17.kv_ref, bf16[512,128]{1,0:T(8,128)(2,1)} %get-tuple-element.10.gate_ref), custom_call_target="tpu_custom_call" | custom-call | tf_op jit(solution)/shard_map/attention/attention/pallas_call | solution.py:267
  188.8 31.1 %all_to_all.27.parts_ref = bf16[8,64,1280]{2,1,0:T(8,128)(2,1)} all-to-all(bf16[8,64,1280]{2,1,0:T(8,128)(2,1)} %attention.1), channel_id=1, replica_groups=mesh['sp'=12,'tp'=8,'dp'=8] {'tp'}, dimensions={0} | all-to-all | bytes 2621440 | tf_op jit(solution)/shard_map/exchange_parts/all_to_all | solution.py:282
  219.9 0.0 all-gather.6.cloned.1.call-done
  219.9 9.0 %finish.1 = bf16[64,3072]{1,0:T(8,128)(2,1)} custom-call(bf16[8,64,1280]{2,1,0:T(8,128)(2,1)} %all_to_all.27.parts_ref, bf16[8,1024,384]{2,1,0:T(8,128)(2,1)} %bitcast.16, f32[96,256]{1,0:T(8,128)} %bitcast.18, f32[1,3072]{1,0:T(1,128)} %bitcast.23, f32[1,128]{1,0:T(1,128)} %bitcast.24), custom_call_target="tpu_custom_call" | custom-call | tf_op jit(solution)/shard_map/finish/finish/pallas_call | solution.py:284
Async XLA Ops:
  6.5 65.4 %copy-start.1 = (bf16[1024,384]{1,0:T(8,128)(2,1)S(1)}, bf16[1024,384]{1,0:T(8,128)(2,1)}, u32[]{:S(2)}) copy-start(bf16[1024,384]{1,0:T(8,128)(2,1)} %param.31) | copy-start | bytes 2359300
  6.5 63.6 %all-gather.8.cloned.1.call-start = ((), (), s32[]{:S(2)}) async-start(), calls=%async_computation.5 | async-start | bytes 3981312 | tf_op jit(solution)/shard_map/gather_rows/all_gather | solution.py:206
  8.5 211.5 %all-gather.6.cloned.1.call-start = ((), (), s32[]{:S(2)}) async-start(), calls=%async_computation.4 | async-start | bytes 7077888 | tf_op jit(solution)/shard_map/gather_out_weight/all_gather | solution.py:217
  71.9 19.2 %copy-start.4 = (bf16[3072,256]{1,0:T(8,128)(2,1)S(1)}, bf16[3072,256]{1,0:T(8,128)(2,1)}, u32[]{:S(2)}) copy-start(bf16[3072,256]{1,0:T(8,128)(2,1)} %param.27) | copy-start | bytes 4718596
  72.9 18.2 %copy-start.5 = (bf16[3072,256]{1,0:T(8,128)(2,1)S(1)}, bf16[3072,256]{1,0:T(8,128)(2,1)}, u32[]{:S(2)}) copy-start(bf16[3072,256]{1,0:T(8,128)(2,1)} %param.26) | copy-start | bytes 4718596
  76.7 29.2 %all-to-all-start = ((f32[96,1,256]{2,1,0:T(1,128)}), f32[96,1,256]{2,1,0:T(1,128)S(1)}, u32[]{:S(2)}, u32[]{:S(2)}) async-start(f32[96,1,256]{2,1,0:T(1,128)} %copy.17), calls=%async_computation | async-start | bytes 196608 | tf_op jit(solution)/shard_map/modulation/all_to_all | solution.py:186
  91.3 21.4 %copy-start.2 = (bf16[3072,128]{1,0:T(8,128)(2,1)S(1)}, bf16[3072,128]{1,0:T(8,128)(2,1)}, u32[]{:S(2)}) copy-start(bf16[3072,128]{1,0:T(8,128)(2,1)} %param.28) | copy-start | bytes 2359300
  91.3 21.4 %copy-start.3 = (bf16[3072,128]{1,0:T(8,128)(2,1)S(1)}, bf16[3072,128]{1,0:T(8,128)(2,1)}, u32[]{:S(2)}) copy-start(bf16[3072,128]{1,0:T(8,128)(2,1)} %param.25) | copy-start | bytes 2359300
  106.7 20.6 %all-to-all-start.1 = ((f32[96,1,256]{2,1,0:T(1,128)}), f32[96,1,256]{2,1,0:T(1,128)S(1)}, u32[]{:S(2)}, u32[]{:S(2)}) async-start(f32[96,1,256]{2,1,0:T(1,128)} %broadcast_in_dim.32), calls=%async_computation.1 | async-start | bytes 196608 | tf_op jit(solution)/shard_map/modulation/all_to_all | solution.py:189
  137.0 5.9 %copy-start.6 = (bf16[136,256]{1,0:T(8,128)(2,1)S(1)}, bf16[136,256]{1,0:T(8,128)(2,1)}, u32[]{:S(2)}) copy-start(bf16[136,256]{1,0:T(8,128)(2,1)} %get-tuple-element.9) | copy-start | bytes 208900
  138.8 32.3 %all-to-all-start.2 = ((bf16[4,512,128]{2,1,0:T(8,128)(2,1)}), bf16[4,512,128]{2,1,0:T(8,128)(2,1)S(1)}, u32[]{:S(2)}, u32[]{:S(2)}) async-start(bf16[4,512,128]{2,1,0:T(8,128)(2,1)} %broadcast_in_dim.34), calls=%async_computation.2 | async-start | bytes 1048576 | tf_op jit(solution)/shard_map/exchange_queries/all_to_all | solution.py:262
  171.1 0.9 copy-start
Sparse Core Ops, SparseCore 0:
  9.7 60.3 all-gather.7
  73.1 89.7 all-gather.5

commit v2 on v1

v2 whole, which is shorter than its diff:
```python
import jax
import jax.numpy as jnp
from jax import lax
from jax.experimental import pallas as pl
from jax.experimental.pallas import tpu as pltpu
from jax.sharding import PartitionSpec as P


D = 3072
GROUP = 4
HQK = 64
HV = 128
ROWS = 64
CTX_ROWS = 4
TP = 8
SP = 12
QUARTER = 2 * (ROWS + CTX_ROWS)
KEYS = SP * QUARTER
MESSAGE = GROUP * 2 * HV + 2 * HV
CHUNK = 256
CHAIN = 512
VECTOR_ROWS = D // CHUNK
SCALE = HQK ** (-0.5) * 1.4426950408889634
NORM_EPSILON = 1e-06
F32 = jnp.float32
BF16 = jnp.bfloat16
TP_GROUPS = [[0, 1, 2, 3], [4, 5, 6, 7]]
CORE_PAIRS = [[0, 1], [2, 3], [4, 5], [6, 7]]
VMEM_LIMIT = 60 * 1024 * 1024


def silu(values):
    return values / (1.0 + jnp.exp(-values))


def partial_sums_kernel(cond_ref, ctx_ref, shift_ref, scale_ref, gate_ref, out_ref):
    both = jnp.concatenate([cond_ref[...], ctx_ref[...]], axis=0).astype(F32)
    both = silu(both).astype(BF16)
    out_ref[...] = jnp.zeros_like(out_ref)
    shift = jnp.dot(both, shift_ref[...], preferred_element_type=F32)
    scale = jnp.dot(both, scale_ref[...], preferred_element_type=F32)
    gate = jnp.dot(both, gate_ref[...], preferred_element_type=F32)
    vectors = [shift[:1], scale[:1], gate[:1], shift[1:], scale[1:]]
    for number, vector in enumerate(vectors):
        for piece in range(VECTOR_ROWS):
            row = number * VECTOR_ROWS + piece
            out_ref[row] = vector[:, piece * CHUNK : (piece + 1) * CHUNK]


def vector_of(sums_ref, number):
    first = number * VECTOR_ROWS
    return jnp.concatenate(
        [sums_ref[first + piece] for piece in range(VECTOR_ROWS)], axis=1
    )


def project_kernel(
    quarter_ref, rows_ref, sums_ref, gain_ref, qg_weight_ref, kv_weight_ref,
    q_ref, gate_ref, kv_ref, latent_ref, context_ref,
):
    step = pl.program_id(0)
    pieces = rows_ref.shape[0]
    gain = gain_ref[...]
    latent_scale = gain * (1.0 + vector_of(sums_ref, 1))
    latent_shift = vector_of(sums_ref, 0)
    context_scale = gain * (1.0 + vector_of(sums_ref, 4))
    context_shift = vector_of(sums_ref, 3)
    for piece in range(pieces):
        number = step * pieces + piece
        values = rows_ref[piece].astype(F32)
        square = jnp.mean(values * values, axis=-1, keepdims=True)
        normed = values * lax.rsqrt(square + NORM_EPSILON)
        latent = normed[:ROWS] * latent_scale + latent_shift
        latent_ref[pl.ds(pl.multiple_of(number * ROWS, ROWS), ROWS), :] = latent.astype(BF16)
        context_ref[number, :CTX_ROWS, :] = normed[ROWS:] * context_scale + context_shift

    @pl.when(step == pl.num_programs(0) - 1)
    def _():
        projected = jnp.dot(latent_ref[...], qg_weight_ref[...], preferred_element_type=F32)
        queries = projected[:, :HV].astype(BF16)
        for copy in range(GROUP):
            q_ref[copy] = queries
        gate_ref[...] = projected[:, HV:].astype(BF16)
        quarter = quarter_ref[0]
        first = pl.multiple_of(quarter * 2 * ROWS, 2 * ROWS)
        kv = jnp.dot(
            latent_ref[pl.ds(first, 2 * ROWS), :], kv_weight_ref[...], preferred_element_type=F32
        )
        kv_ref[: 2 * ROWS, :] = kv.astype(BF16)
        own_context = jnp.concatenate(
            [context_ref[2 * quarter, :CTX_ROWS, :], context_ref[2 * quarter + 1, :CTX_ROWS, :]],
            axis=0,
        ).astype(BF16)
        kv = jnp.dot(own_context, kv_weight_ref[...], preferred_element_type=F32)
        kv_ref[2 * ROWS :, :] = kv.astype(BF16)


def three_parts(value):
    high = value.astype(BF16)
    rest = value - high.astype(F32)
    middle = rest.astype(BF16)
    low = (rest - middle.astype(F32)).astype(BF16)
    return high.astype(F32), middle.astype(F32), low.astype(F32)


def attention_kernel(lambda_ref, q_ref, kv_ref, gate_ref, out_ref):
    peers = out_ref.shape[0]
    block = peers * ROWS
    q = q_ref[...].reshape(GROUP * block, 2 * HQK)
    keys = kv_ref[:, : 2 * HQK]
    value_rows = kv_ref[:, 2 * HQK :]
    lane = lax.broadcasted_iota(jnp.int32, (CHAIN, 2 * HQK), 1)
    chains = [(first, m) for first in range(0, GROUP * block, CHAIN) for m in range(2)]

    def scores_of(first, m):
        rows = q[first : first + CHAIN]
        rows = jnp.where(lane // HQK == m, rows, jnp.zeros_like(rows))
        return lax.dot_general(rows, keys, (((1,), (1,)), ((), ())), preferred_element_type=F32)

    def exponent_of(scores):
        largest = jnp.max(scores, axis=-1, keepdims=True) * SCALE
        exponent = jnp.exp2(scores * SCALE - largest)
        return exponent.astype(BF16), jnp.sum(exponent, axis=-1, keepdims=True), largest

    def ratio_of(weights, total, largest):
        weighted = jnp.dot(weights, value_rows, preferred_element_type=F32)
        return (weighted / total).astype(BF16), largest + jnp.log2(total)

    ahead, waiting, ratios, levels = scores_of(*chains[0]), None, {}, {}

    def settle():
        first, m = waiting[0]
        ratio, level = ratio_of(*waiting[1])
        for inner in range(0, CHAIN, block):
            head = (first + inner) // block
            ratios[head, m] = ratio[inner : inner + block]
            levels[head, m] = level[inner : inner + block]

    for number, chain in enumerate(chains):
        scores = ahead
        if number + 1 < len(chains):
            ahead = scores_of(*chains[number + 1])
        exponent = exponent_of(scores)
        if waiting is not None:
            settle()
        waiting = (chain, exponent)
    settle()

    stat_lane = lax.broadcasted_iota(jnp.int32, (block, HV), 1)
    stats = jnp.zeros((block, HV), F32)
    for part, piece in enumerate(three_parts(jnp.full((block, HV), lambda_ref[0], F32))):
        stats = jnp.where(stat_lane == part * 32 + 2 * GROUP, piece, stats)
    for (head, m), ratio in ratios.items():
        column = (2 * head + m) * HV
        for p in range(peers):
            out_ref[p, :, column : column + HV] = ratio[p * ROWS : (p + 1) * ROWS]
        wide = jnp.broadcast_to(levels[head, m], (block, HV))
        for part, piece in enumerate(three_parts(wide)):
            stats = jnp.where(stat_lane == part * 32 + 2 * head + m, piece, stats)
    for p in range(peers):
        out_ref[p, :, 2 * GROUP * HV : 2 * GROUP * HV + HV] = gate_ref[p * ROWS : (p + 1) * ROWS, :]
        out_ref[p, :, 2 * GROUP * HV + HV :] = stats[p * ROWS : (p + 1) * ROWS].astype(BF16)


def finish_kernel(
    parts_ref, weight_ref, sums_ref, post_gain_ref, head_gain_ref, out_ref, branch_ref, projected_ref
):
    step = pl.program_id(0)

    @pl.when(step == 0)
    def _():
        gate_column = 2 * GROUP * HV
        levels = []
        for t in range(TP):
            stats = parts_ref[t, :, gate_column + HV :].astype(F32)
            levels.append(stats[:, :32] + stats[:, 32:64] + stats[:, 64:96])
        for g in range(TP // GROUP):
            members = range(g * GROUP, (g + 1) * GROUP)
            top = levels[members[0]]
            for t in members[1:]:
                top = jnp.maximum(top, levels[t])
            shares = [jnp.exp2(levels[t] - top) for t in members]
            total = shares[0] + shares[1] + shares[2] + shares[3]
            shares = [share / total for share in shares]
            for j in range(GROUP):
                head = g * GROUP + j
                ratios = []
                for m in range(2):
                    index = 2 * j + m
                    ratio = jnp.zeros((ROWS, HV), F32)
                    for t, share in zip(members, shares):
                        part = parts_ref[t, :, index * HV : (index + 1) * HV].astype(F32)
                        ratio = ratio + share[:, index : index + 1] * part
                    ratios.append(ratio)
                own_lambda = levels[head][:, 2 * GROUP : 2 * GROUP + 1]
                attended = ratios[0] - own_lambda * ratios[1]
                square = jnp.mean(attended * attended, axis=-1, keepdims=True)
                gate = parts_ref[head, :, gate_column : gate_column + HV].astype(F32)
                branch = attended * lax.rsqrt(square + NORM_EPSILON) * head_gain_ref[...] * silu(gate)
                branch_ref[:, head * HV : (head + 1) * HV] = branch.astype(BF16)

    half = weight_ref.shape[2]
    pieces = weight_ref.shape[1]
    for piece in range(pieces):
        projected = jnp.dot(branch_ref[:, :half], weight_ref[0, piece], preferred_element_type=F32)
        projected = projected + jnp.dot(
            branch_ref[:, half:], weight_ref[1, piece], preferred_element_type=F32
        )
        projected_ref[step * pieces + piece] = projected.astype(BF16).astype(F32)

    @pl.when(step == pl.num_programs(0) - 1)
    def _():
        square = jnp.zeros((ROWS, 1), F32)
        for t in range(TP):
            square = square + jnp.sum(projected_ref[t] * projected_ref[t], axis=-1, keepdims=True)
        factor = lax.rsqrt(square / D + NORM_EPSILON)
        out_gate = vector_of(sums_ref, 2)
        gain = post_gain_ref[...]
        width = D // TP
        for t in range(TP):
            columns = slice(t * width, (t + 1) * width)
            value = projected_ref[t] * factor * gain[:, columns] * out_gate[:, columns]
            out_ref[:, columns] = value.astype(BF16)


def summed(partials):
    axes = ("sp", "tp")
    pieces = lax.all_to_all(partials, axes, split_axis=0, concat_axis=0, tiled=True)
    own = jnp.sum(pieces, axis=0, keepdims=True)
    copies = jnp.broadcast_to(own, pieces.shape)
    return lax.all_to_all(copies, axes, split_axis=0, concat_axis=0, tiled=True)


def whole_block(shape):
    return pl.BlockSpec(shape, lambda *_: (0,) * len(shape))


def compute(
    latents, condition, context, context_cond, shift_weight, scale_weight, out_gate_weight,
    pre_gain, post_gain, query_weight, key_weight, value_weight, head_gate_weight,
    lambdas, head_gain, out_weight,
):
    params = pltpu.CompilerParams(vmem_limit_bytes=VMEM_LIMIT)
    t = lax.axis_index("tp")
    key_group, quarter = t // GROUP, t % GROUP
    rows = jnp.concatenate([latents[0], context[0]], axis=0)
    rows = lax.all_gather(rows, "tp", axis=0, tiled=False)
    partials = pl.pallas_call(
        partial_sums_kernel,
        out_shape=jax.ShapeDtypeStruct((SP * TP, 1, CHUNK), F32),
        compiler_params=params,
        name="partial_sums",
    )(condition, context_cond[None, :], shift_weight, scale_weight, out_gate_weight)
    sums = summed(partials)
    core = lax.axis_index("dp") % 2
    half = lax.dynamic_slice_in_dim(out_weight, core * GROUP * HV, GROUP * HV, 0)
    half = half + (sums[0, 0, 0] * 0.0).astype(BF16)
    halves = lax.all_gather(half, "tp", axis=0, tiled=False)
    out_weights = lax.all_gather(halves, "dp", axis=0, tiled=False, axis_index_groups=CORE_PAIRS)
    qg_weight = jnp.concatenate([query_weight, head_gate_weight], axis=1)
    kv_weight = jnp.concatenate(
        [
            lax.dynamic_slice_in_dim(key_weight, key_group * 2 * HQK, 2 * HQK, 1),
            lax.dynamic_slice_in_dim(value_weight, key_group * HV, HV, 1),
        ],
        axis=1,
    )
    per_device = ROWS + CTX_ROWS
    queries, head_gate, key_values = pl.pallas_call(
        project_kernel,
        grid_spec=pltpu.PrefetchScalarGridSpec(
            num_scalar_prefetch=1,
            grid=(TP // 2,),
            in_specs=[
                pl.BlockSpec((2, per_device, D), lambda i, _: (i, 0, 0)),
                whole_block((SP * TP, 1, CHUNK)),
                whole_block((1, D)),
                whole_block((D, 2 * HV)),
                whole_block((D, 2 * HV)),
            ],
            out_specs=[
                whole_block((GROUP, TP * ROWS, HV)),
                whole_block((TP * ROWS, HV)),
                whole_block((QUARTER, 2 * HV)),
            ],
            scratch_shapes=[
                pltpu.VMEM((TP * ROWS, D), BF16),
                pltpu.VMEM((TP, 2 * CTX_ROWS, D), F32),
            ],
        ),
        out_shape=[
            jax.ShapeDtypeStruct((GROUP, TP * ROWS, HV), BF16),
            jax.ShapeDtypeStruct((TP * ROWS, HV), BF16),
            jax.ShapeDtypeStruct((QUARTER, 2 * HV), BF16),
        ],
        compiler_params=params,
        name="project",
    )(quarter.astype(jnp.int32)[None], rows, sums, pre_gain[None, :], qg_weight, kv_weight)
    key_values = lax.all_gather(key_values, "sp", axis=0, tiled=True)
    queries = lax.all_to_all(
        queries, "tp", split_axis=0, concat_axis=0, axis_index_groups=TP_GROUPS, tiled=True
    )
    peers = 4
    parts = pl.pallas_call(
        attention_kernel,
        grid=(TP // peers,),
        in_specs=[
            pl.BlockSpec(memory_space=pltpu.SMEM),
            pl.BlockSpec((GROUP, peers * ROWS, HV), lambda i: (0, i, 0)),
            whole_block((KEYS, 2 * HV)),
            pl.BlockSpec((peers * ROWS, HV), lambda i: (i, 0)),
        ],
        out_specs=pl.BlockSpec((peers, ROWS, MESSAGE), lambda i: (i, 0, 0)),
        out_shape=jax.ShapeDtypeStruct((TP, ROWS, MESSAGE), BF16),
        compiler_params=params,
        name="attention",
    )(lambdas, queries, key_values, head_gate)
    parts = lax.all_to_all(parts, "tp", split_axis=0, concat_axis=0, tiled=True)
    mixed_out = pl.pallas_call(
        finish_kernel,
        grid=(TP // 2,),
        in_specs=[
            whole_block((TP, ROWS, MESSAGE)),
            pl.BlockSpec((2, 2, GROUP * HV, D // TP), lambda i: (0, i, 0, 0)),
            whole_block((SP * TP, 1, CHUNK)),
            whole_block((1, D)),
            whole_block((1, HV)),
        ],
        out_specs=whole_block((ROWS, D)),
        out_shape=jax.ShapeDtypeStruct((ROWS, D), BF16),
        scratch_shapes=[
            pltpu.VMEM((ROWS, GROUP * 2 * HV), BF16),
            pltpu.VMEM((TP, ROWS, D // TP), F32),
        ],
        compiler_params=params,
        name="finish",
    )(parts, out_weights, sums, post_gain[None, :], head_gain[None, :])
    return mixed_out[None]


def solution(mesh):
    tokens = P("dp", ("sp", "tp"), None)
    channels = P(("sp", "tp"), None)
    return jax.shard_map(
        compute,
        mesh=mesh,
        in_specs=(
            tokens, P("dp", ("sp", "tp")), tokens, P(("sp", "tp")), channels, channels, channels,
            P(), P(), P(None, "tp"), P(), P(), P(None, "tp"), P("tp"), P(), P(None, "tp"),
        ),
        out_specs=tokens,
        check_vma=False,
    )
```

time: 236 us -> 270 us (1.14)
  blocking collectives: 59.3 us -> 102 us
  waiting for transfers between devices: 88.2 us -> 103 us
  starting transfers between devices: 23.8 us -> 10.5 us
  Pallas kernels: 36.9 us -> 29.7 us
    all_to_all x1 -> x2, blocking collectives: 31.1 us -> 70.8 us  [the longest x1 37 us: summed(): lax.all_to_all(partials, axes, split_axis=0, concat_axis=0, tiled=True)]
    all_gather x2 -> x3, waiting for transfers between devices: 61.6 us -> 88.7 us  [the longest x1 49.7 us: compute(): rows = lax.all_gather(rows, 'tp', axis=0, tiled=False)]
    all_to_all x2 -> x1, starting transfers between devices: 17.9 us -> 4.43 us  [compute(): lax.all_to_all(queries, 'tp', split_axis=0, concat_axis=0, axis_index_gro...]
    all_to_all x2 -> x1, waiting for transfers between devices: 13.3 us -> 0.01 us  [compute(): lax.all_to_all(queries, 'tp', split_axis=0, concat_axis=0, axis_index_gro...]
    pallas_call x4, Pallas kernels: 36.9 us -> 29.7 us  [the longest x1 13 us: compute(): pl.pallas_call(attention_kernel, grid=(TP // peers,), in_specs=[pl.BlockS...]
    all_gather x1, blocking collectives: 28.2 us -> 31.5 us  [compute(): key_values = lax.all_gather(key_values, 'sp', axis=0, tiled=True)]
  transfers between devices with their start and end apart: 5 -> 5, of which waited for: 3 -> 3; matrix products, arithmetic and copies ran while one was open for 3% -> 1% of each run, Pallas kernels for 12% -> 8%
where the time goes in v2:
time: 270 us; the launch traced here: 269 us
  waiting for transfers between devices  103 us (38%)
  blocking collectives  102 us (38%)
  Pallas kernels  29.7 us (11%)
  between operations  14.5 us (5%)
  starting transfers between devices  10.5 us (4%)
  local copies, waits for them, and re-layouts  4.54 us (2%)
  other arithmetic  4.44 us (2%)
    all_gather x1, waiting for transfers between devices, compute(): rows = lax.all_gather(rows, 'tp', axis=0, tiled=False)  49.7 us
    all_gather x1, waiting for transfers between devices, compute(): halves = lax.all_gather(half, 'tp', axis=0, tiled=False)  39 us
    all_to_all x1, blocking collectives, summed(): lax.all_to_all(partials, axes, split_axis=0, concat_axis=0, tiled=True)  37 us
    all_to_all x1, blocking collectives, compute(): parts = lax.all_to_all(parts, 'tp', split_axis=0, concat_axis=0, tiled=True)  33.8 us
    all_gather x1, blocking collectives, compute(): key_values = lax.all_gather(key_values, 'sp', axis=0, tiled=True)  31.5 us
    all_to_all x1, waiting for transfers between devices, summed(): return lax.all_to_all(copies, axes, split_axis=0, concat_axis=0, tiled=True)  14.6 us
    pallas_call x1, Pallas kernels, compute(): pl.pallas_call(attention_kernel, grid=(TP // peers,), in_specs=[pl.BlockS...  13 us
    pallas_call x1, Pallas kernels, compute(): pl.pallas_call(project_kernel, grid_spec=pltpu.PrefetchScalarGridSpec(num...  7.53 us
  transfers between devices with their start and end apart: 5, of which 3 were waited for; matrix products, arithmetic and copies ran while one was open for 1% of the time, Pallas kernels for 8%

profile of v2, /device:TPU:2, one launch (start us, length us, event | category | flops | bytes accessed | tf_op | source)
XLA Modules:
  0.0 269.4 jit_solution(3675964655560925160)
XLA Ops:
  6.5 0.0 copy-start.7
  6.5 0.0 copy-start.4
  6.5 0.0 copy-start.8
  6.5 2.1 partial_sums.1
  8.7 37.0 %all_to_all.20 = f32[96,1,256]{2,1,0:T(1,128)S(1)} all-to-all(f32[96,1,256]{2,1,0:T(1,128)} %partial_sums.1), channel_id=1, replica_groups=mesh['sp'=12,'tp'=8,'dp'=8] {'sp','tp'}, dimensions={0} | all-to-all | bytes 196608 | tf_op jit(solution)/shard_map/all_to_all | solution.py:228
  45.6 0.1 reduce_sum.9
  45.8 0.7 broadcast_in_dim.26
  46.5 5.9 %all-to-all-start.1 = ((f32[96,1,256]{2,1,0:T(1,128)}), f32[96,1,256]{2,1,0:T(1,128)S(1)}, u32[]{:S(2)}, u32[]{:S(2)}) async-start(f32[96,1,256]{2,1,0:T(1,128)} %broadcast_in_dim.26), calls=%async_computation.1 | async-start | bytes 196608 | tf_op jit(solution)/shard_map/all_to_all | solution.py:231
  52.4 0.0 all-gather.8.cloned.1.call-start
  52.5 14.6 %all-to-all-done.1.sums_ref = f32[96,1,256]{2,1,0:T(1,128)S(1)} async-done(((f32[96,1,256]{2,1,0:T(1,128)}), f32[96,1,256]{2,1,0:T(1,128)S(1)}, u32[]{:S(2)}, u32[]{:S(2)}) %all-to-all-start.1) | async-done | bytes 98336 | tf_op jit(solution)/shard_map/all_to_all | solution.py:231
  67.0 0.0 copy-start.1
  67.0 0.5 slice.4
  68.2 0.0 copy-done.7
  68.3 0.8 dynamic-slice_add_fusion
  69.1 0.0 all-gather.8.cloned.1.call-update
  69.1 0.0 all-gather.12.cloned.1.call-start
  69.2 0.0 copy-done.4
  69.2 0.0 copy-done.8
  69.2 0.8 maximum_bitcast_fusion
  70.0 0.0 all-gather.12.cloned.1.call-update
  70.0 0.0 all-gather.10.cloned.1.call-start
  70.1 39.0 %all-gather.8.cloned.1.call-done = bf16[4096,384]{1,0:T(8,128)(2,1)} async-done(((bf16[512,384]{1,0:T(8,128)(2,1)}), bf16[4096,384]{1,0:T(8,128)(2,1)}) %all-gather.8.cloned.1.call-update) | async-done | bytes 3145744 | tf_op jit(solution)/shard_map/all_gather | solution.py:258
  109.1 0.0 copy-start.5
  109.1 0.0 copy-start.6
  109.1 0.0 all-gather.10.cloned.1.call-update
  109.1 0.0 copy-done.1
  109.1 1.3 copy-done.5
  110.5 0.5 copy-done.6
  110.9 0.1 constant_dynamic-slice_fusion
  111.0 0.0 copy-start.2
  111.1 0.0 copy-start.3
  111.1 1.3 pad_maximum_fusion.1.kv_weight_ref
  112.4 0.0 copy-done.2
  112.4 0.6 copy-done.3
  113.0 1.3 pad_maximum_fusion.qg_weight_ref
  114.3 49.7 %all-gather.12.cloned.1.call-done.rows_ref = bf16[8,68,3072]{2,1,0:T(8,128)(2,1)} async-done(((bf16[1,68,3072]{2,1,0:T(8,128)(2,1)}), bf16[8,68,3072]{2,1,0:T(8,128)(2,1)}) %all-gather.12.cloned.1.call-update) | async-done | bytes 3342352 | tf_op jit(solution)/shard_map/all_gather | solution.py:247
  164.1 7.5 %project.1 = (bf16[4,512,128]{2,1,0:T(8,128)(2,1)}, bf16[512,128]{1,0:T(8,128)(2,1)}, bf16[136,256]{1,0:T(8,128)(2,1)}) custom-call(s32[1]{0:T(128)} %bitcast.quarter_ref, bf16[8,68,3072]{2,1,0:T(8,128)(2,1)} %all-gather.12.cloned.1.call-done.rows_ref, f32[96,1,256]{2,1,0:T(1,128)} %copy-done.1, f32[1,3072]{1,0:T(1,128)} %bitcast.17, ...), custom_call_target="tpu_custom_call" | custom-call | tf_op jit(solution)/shard_map/project/pallas_call | solution.py:269
  171.6 4.4 %all-to-all-start.2 = ((bf16[4,512,128]{2,1,0:T(8,128)(2,1)}), bf16[4,512,128]{2,1,0:T(8,128)(2,1)S(1)}, u32[]{:S(2)}, u32[]{:S(2)}) async-start(bf16[4,512,128]{2,1,0:T(8,128)(2,1)} %get-tuple-element.8), calls=%async_computation.2 | async-start | bytes 1048576 | tf_op jit(solution)/shard_map/all_to_all | solution.py:300
  176.7 31.5 %all_gather.23.kv_ref = bf16[1632,256]{1,0:T(8,128)(2,1)} all-gather(bf16[136,256]{1,0:T(8,128)(2,1)} %get-tuple-element.9), channel_id=1, replica_groups=mesh['sp'=12,'tp'=8,'dp'=8] {'sp'}, dimensions={0}, use_global_device_ids=true | all-gather | bytes 905216 | tf_op jit(solution)/shard_map/all_gather | solution.py:299
  208.2 0.0 all-to-all-done.2.q_ref
  208.2 0.0 copy-start
  208.2 0.8 copy-done
  209.0 13.0 %attention.1 = bf16[8,64,1280]{2,1,0:T(8,128)(2,1)} custom-call(f32[1]{0:T(128)S(6)} %copy.17.lambda_ref, bf16[4,512,128]{2,1,0:T(8,128)(2,1)} %copy-done, bf16[1632,256]{1,0:T(8,128)(2,1)} %all_gather.23.kv_ref, bf16[512,128]{1,0:T(8,128)(2,1)} %get-tuple-element.10.gate_ref), custom_call_target="tpu_custom_call" | custom-call | tf_op jit(solution)/shard_map/attention/pallas_call | solution.py:304
  222.0 33.8 %all_to_all.21.parts_ref = bf16[8,64,1280]{2,1,0:T(8,128)(2,1)} all-to-all(bf16[8,64,1280]{2,1,0:T(8,128)(2,1)} %attention.1), channel_id=1, replica_groups=mesh['sp'=12,'tp'=8,'dp'=8] {'tp'}, dimensions={0} | all-to-all | bytes 2621440 | tf_op jit(solution)/shard_map/all_to_all | solution.py:318
  255.8 0.0 all-gather.10.cloned.1.call-done
  255.8 7.0 %finish.1 = bf16[64,3072]{1,0:T(8,128)(2,1)} custom-call(bf16[8,64,1280]{2,1,0:T(8,128)(2,1)} %all_to_all.21.parts_ref, bf16[2,8,512,384]{3,2,1,0:T(8,128)(2,1)} %bitcast.13, f32[96,1,256]{2,1,0:T(1,128)} %copy-done.1, f32[1,3072]{1,0:T(1,128)} %bitcast.18, f32[1,128]{1,0:T(1,128)} %bitcast.19), custom_call_target="tpu_custom_call" | custom-call | tf_op jit(solution)/shard_map/finish/pallas_call | solution.py:319
Async XLA Ops:
  6.5 61.7 %copy-start.7 = (bf16[1024,384]{1,0:T(8,128)(2,1)S(1)}, bf16[1024,384]{1,0:T(8,128)(2,1)}, u32[]{:S(2)}) copy-start(bf16[1024,384]{1,0:T(8,128)(2,1)} %param.31) | copy-start | bytes 2359300
  6.5 62.6 %copy-start.4 = (bf16[1,64,3072]{2,1,0:T(8,128)(2,1)S(1)}, bf16[1,64,3072]{2,1,0:T(8,128)(2,1)}, u32[]{:S(2)}) copy-start(bf16[1,64,3072]{2,1,0:T(8,128)(2,1)} %param.16) | copy-start | bytes 1179652
  6.5 62.6 %copy-start.8 = (bf16[1,4,3072]{2,1,0:T(4,128)(2,1)S(1)}, bf16[1,4,3072]{2,1,0:T(4,128)(2,1)}, u32[]{:S(2)}) copy-start(bf16[1,4,3072]{2,1,0:T(4,128)(2,1)} %param.18) | copy-start | bytes 73732
  46.5 20.6 %all-to-all-start.1 = ((f32[96,1,256]{2,1,0:T(1,128)}), f32[96,1,256]{2,1,0:T(1,128)S(1)}, u32[]{:S(2)}, u32[]{:S(2)}) async-start(f32[96,1,256]{2,1,0:T(1,128)} %broadcast_in_dim.26), calls=%async_computation.1 | async-start | bytes 196608 | tf_op jit(solution)/shard_map/all_to_all | solution.py:231
  52.4 56.6 %all-gather.8.cloned.1.call-start = ((), (), s32[]{:S(2)}) async-start(), calls=%async_computation.4 | async-start | bytes 3538944 | tf_op jit(solution)/shard_map/all_gather | solution.py:258
  67.0 42.0 %copy-start.1 = (f32[96,1,256]{2,1,0:T(1,128)}, f32[96,1,256]{2,1,0:T(1,128)S(1)}, u32[]{:S(2)}) copy-start(f32[96,1,256]{2,1,0:T(1,128)S(1)} %all-to-all-done.1.sums_ref) | copy-start | bytes 294916
  69.1 95.0 %all-gather.12.cloned.1.call-start = ((), (), s32[]{:S(2)}) async-start(), calls=%async_computation.6 | async-start | bytes 3981312 | tf_op jit(solution)/shard_map/all_gather | solution.py:247
  70.0 185.8 %all-gather.10.cloned.1.call-start = ((), (), s32[]{:S(2)}) async-start(), calls=%async_computation.5 | async-start | bytes 9437184 | tf_op jit(solution)/shard_map/all_gather | solution.py:259
  109.1 1.4 copy-start.5
  109.1 1.9 copy-start.6
  111.0 1.4 copy-start.2
  111.1 1.9 copy-start.3
  171.6 36.6 %all-to-all-start.2 = ((bf16[4,512,128]{2,1,0:T(8,128)(2,1)}), bf16[4,512,128]{2,1,0:T(8,128)(2,1)S(1)}, u32[]{:S(2)}, u32[]{:S(2)}) async-start(bf16[4,512,128]{2,1,0:T(8,128)(2,1)} %get-tuple-element.8), calls=%async_computation.2 | async-start | bytes 1048576 | tf_op jit(solution)/shard_map/all_to_all | solution.py:300
  208.2 0.8 copy-start
Sparse Core Ops, SparseCore 0:
  69.2 39.7 all-gather.7
  111.4 52.5 all-gather.11
  166.4 26.6 all-gather.9

commit v3 on v2

v3 whole, which is shorter than its diff:
```python
import jax
import jax.numpy as jnp
from jax import lax
from jax.experimental import pallas as pl
from jax.experimental.pallas import tpu as pltpu
from jax.sharding import PartitionSpec as P


D = 3072
GROUP = 4
HQK = 64
HV = 128
ROWS = 64
CTX_ROWS = 4
TP = 8
SP = 12
QUARTER = 2 * (ROWS + CTX_ROWS)
KEYS = SP * QUARTER
STATS = GROUP * 2
GATE_ROW = STATS * ROWS
STAT_ROW = GATE_ROW + ROWS
MESSAGE = STAT_ROW + 2 * STATS
CHUNK = 256
CHAIN = 512
VECTOR_ROWS = D // CHUNK
SCALE = HQK ** (-0.5) * 1.4426950408889634
NORM_EPSILON = 1e-06
F32 = jnp.float32
BF16 = jnp.bfloat16
TP_GROUPS = [[0, 1, 2, 3], [4, 5, 6, 7]]
VMEM_LIMIT = 60 * 1024 * 1024


def silu(values):
    return values / (1.0 + jnp.exp(-values))


def partial_sums_kernel(cond_ref, ctx_ref, shift_ref, scale_ref, gate_ref, out_ref):
    both = jnp.concatenate([cond_ref[...], ctx_ref[...]], axis=0).astype(F32)
    both = silu(both).astype(BF16)
    out_ref[...] = jnp.zeros_like(out_ref)
    shift = jnp.dot(both, shift_ref[...], preferred_element_type=F32)
    scale = jnp.dot(both, scale_ref[...], preferred_element_type=F32)
    gate = jnp.dot(both, gate_ref[...], preferred_element_type=F32)
    vectors = [shift[:1], scale[:1], gate[:1], shift[1:], scale[1:]]
    for number, vector in enumerate(vectors):
        for piece in range(VECTOR_ROWS):
            row = number * VECTOR_ROWS + piece
            out_ref[row] = vector[:, piece * CHUNK : (piece + 1) * CHUNK]


def vector_of(sums_ref, number):
    first = number * VECTOR_ROWS
    return jnp.concatenate(
        [sums_ref[first + piece] for piece in range(VECTOR_ROWS)], axis=1
    )


def modulated(tokens, scale, shift):
    values = tokens.astype(F32)
    square = jnp.mean(values * values, axis=-1, keepdims=True)
    return (values * lax.rsqrt(square + NORM_EPSILON) * scale + shift).astype(BF16)


def project_kernel(
    place_ref, rows_ref, own_ref, other_ref, sums_ref, gain_ref,
    query_weight_ref, gate_weight_ref, key_weight_ref, value_weight_ref,
    q_ref, gate_ref, kv_ref, latent_ref,
):
    step = pl.program_id(0)
    pieces = rows_ref.shape[0]
    gain = gain_ref[...]
    scale, shift = gain * (1.0 + vector_of(sums_ref, 1)), vector_of(sums_ref, 0)
    for piece in range(pieces):
        first = pl.multiple_of((step * pieces + piece) * ROWS, ROWS)
        latent_ref[pl.ds(first, ROWS), :] = modulated(rows_ref[piece], scale, shift)

    @pl.when(step == pl.num_programs(0) - 1)
    def _():
        weight = jnp.concatenate([query_weight_ref[...], gate_weight_ref[...]], axis=1)
        projected = jnp.dot(latent_ref[...], weight, preferred_element_type=F32)
        queries = projected[:, :HV].astype(BF16)
        for copy in range(GROUP):
            q_ref[copy] = queries
        gate_ref[...] = projected[:, HV:].astype(BF16)
        weight = jnp.concatenate([key_weight_ref[...], value_weight_ref[...]], axis=1)
        first = pl.multiple_of(place_ref[0] * 2 * ROWS, 2 * ROWS)
        kv = jnp.dot(latent_ref[pl.ds(first, 2 * ROWS), :], weight, preferred_element_type=F32)
        kv_ref[: 2 * ROWS, :] = kv.astype(BF16)
        context = jnp.concatenate([own_ref[...].astype(F32), other_ref[...].astype(F32)], axis=0)
        context_scale = gain * (1.0 + vector_of(sums_ref, 4))
        context = modulated(context, context_scale, vector_of(sums_ref, 3))
        kv = jnp.dot(context, weight, preferred_element_type=F32)
        kv_ref[2 * ROWS :, :] = kv.astype(BF16)


def three_parts(value):
    high = value.astype(BF16)
    rest = value - high.astype(F32)
    middle = rest.astype(BF16)
    low = (rest - middle.astype(F32)).astype(BF16)
    return high.astype(F32), middle.astype(F32), low.astype(F32)


def attention_kernel(lambda_ref, q_ref, kv_ref, gate_ref, out_ref):
    peers = out_ref.shape[0]
    block = peers * ROWS
    q = q_ref[...].reshape(GROUP * block, 2 * HQK)
    keys = kv_ref[:, : 2 * HQK]
    value_rows = kv_ref[:, 2 * HQK :]
    lane = lax.broadcasted_iota(jnp.int32, (CHAIN, 2 * HQK), 1)
    chains = [(first, m) for first in range(0, GROUP * block, CHAIN) for m in range(2)]

    def scores_of(first, m):
        rows = q[first : first + CHAIN]
        rows = jnp.where(lane // HQK == m, rows, jnp.zeros_like(rows))
        return lax.dot_general(rows, keys, (((1,), (1,)), ((), ())), preferred_element_type=F32)

    def exponent_of(scores):
        largest = jnp.max(scores, axis=-1, keepdims=True) * SCALE
        exponent = jnp.exp2(scores * SCALE - largest)
        return exponent.astype(BF16), jnp.sum(exponent, axis=-1, keepdims=True), largest

    def ratio_of(weights, total, largest):
        weighted = jnp.dot(weights, value_rows, preferred_element_type=F32)
        return (weighted / total).astype(BF16), largest + jnp.log2(total)

    ahead, waiting, ratios, levels = scores_of(*chains[0]), None, {}, {}

    def settle():
        first, m = waiting[0]
        ratio, level = ratio_of(*waiting[1])
        for inner in range(0, CHAIN, block):
            head = (first + inner) // block
            ratios[head, m] = ratio[inner : inner + block]
            levels[head, m] = level[inner : inner + block]

    for number, chain in enumerate(chains):
        scores = ahead
        if number + 1 < len(chains):
            ahead = scores_of(*chains[number + 1])
        exponent = exponent_of(scores)
        if waiting is not None:
            settle()
        waiting = (chain, exponent)
    settle()

    stat_lane = lax.broadcasted_iota(jnp.int32, (block, HV), 1)
    stats = jnp.zeros((block, HV), F32)
    for (head, m), ratio in ratios.items():
        index = 2 * head + m
        for p in range(peers):
            out_ref[p, index * ROWS : (index + 1) * ROWS, :] = ratio[p * ROWS : (p + 1) * ROWS]
        wide = jnp.broadcast_to(levels[head, m], (block, HV))
        stats = jnp.where(stat_lane == index, wide, stats)
    high, middle, low = three_parts(jnp.transpose(stats)[:STATS])
    row = lax.broadcasted_iota(jnp.int32, (STATS, ROWS), 0)
    own_lambda = jnp.zeros((STATS, ROWS), F32)
    for part, piece in enumerate(three_parts(jnp.full((STATS, ROWS), lambda_ref[0], F32))):
        own_lambda = jnp.where(row == part, piece, own_lambda)
    for p in range(peers):
        lanes = slice(p * ROWS, (p + 1) * ROWS)
        out_ref[p, GATE_ROW:STAT_ROW, :] = gate_ref[lanes, :]
        upper = jnp.concatenate([high[:, lanes], middle[:, lanes]], axis=1)
        lower = jnp.concatenate([low[:, lanes], own_lambda], axis=1)
        out_ref[p, STAT_ROW:, :] = jnp.concatenate([upper, lower], axis=0).astype(BF16)


def finish_kernel(
    core_ref, parts_ref, own_ref, other_ref, sums_ref, post_gain_ref, head_gain_ref,
    out_ref, branch_ref, projected_ref,
):
    step = pl.program_id(0)

    @pl.when(step == 0)
    def _():
        levels, lambdas = [], []
        for t in range(TP):
            stats = parts_ref[t, STAT_ROW:, :].astype(F32)
            upper, lower = stats[:STATS], stats[STATS:]
            levels.append(upper[:, :ROWS] + upper[:, ROWS:] + lower[:, :ROWS])
            lambdas.append(lower[0:1, ROWS:] + lower[1:2, ROWS:] + lower[2:3, ROWS:])
        shares = []
        for g in range(TP // GROUP):
            group = levels[g * GROUP : (g + 1) * GROUP]
            top = jnp.maximum(jnp.maximum(group[0], group[1]), jnp.maximum(group[2], group[3]))
            group = [jnp.exp2(level - top) for level in group]
            total = group[0] + group[1] + group[2] + group[3]
            shares = shares + [share / total for share in group]
        columns = jnp.concatenate(shares + lambdas, axis=0)
        columns = jnp.concatenate([columns, jnp.zeros_like(columns)], axis=1)
        columns = jnp.concatenate(
            [columns, jnp.zeros((HV - columns.shape[0], HV), F32)], axis=0
        )
        columns = jnp.transpose(columns)[:ROWS]
        for head in range(TP):
            g, j = head // GROUP, head % GROUP
            ratios = []
            for m in range(2):
                index = 2 * j + m
                ratio = jnp.zeros((ROWS, HV), F32)
                for t in range(g * GROUP, (g + 1) * GROUP):
                    part = parts_ref[t, index * ROWS : (index + 1) * ROWS, :].astype(F32)
                    column = t * STATS + index
                    ratio = ratio + columns[:, column : column + 1] * part
                ratios.append(ratio)
            column = TP * STATS + head
            attended = ratios[0] - columns[:, column : column + 1] * ratios[1]
            square = jnp.mean(attended * attended, axis=-1, keepdims=True)
            gate = parts_ref[head, GATE_ROW:STAT_ROW, :].astype(F32)
            branch = attended * lax.rsqrt(square + NORM_EPSILON) * head_gain_ref[...] * silu(gate)
            branch_ref[g, :, j * HV : (j + 1) * HV] = branch.astype(BF16)

    own = core_ref[0]
    pieces = own_ref.shape[0]
    for piece in range(pieces):
        projected = jnp.dot(branch_ref[own], own_ref[piece], preferred_element_type=F32)
        projected = projected + jnp.dot(
            branch_ref[1 - own], other_ref[piece], preferred_element_type=F32
        )
        projected_ref[step * pieces + piece] = projected.astype(BF16).astype(F32)

    @pl.when(step == pl.num_programs(0) - 1)
    def _():
        square = jnp.zeros((ROWS, 1), F32)
        for t in range(TP):
            square = square + jnp.sum(projected_ref[t] * projected_ref[t], axis=-1, keepdims=True)
        factor = lax.rsqrt(square / D + NORM_EPSILON)
        out_gate = vector_of(sums_ref, 2)
        gain = post_gain_ref[...]
        width = D // TP
        for t in range(TP):
            columns = slice(t * width, (t + 1) * width)
            value = projected_ref[t] * factor * gain[:, columns] * out_gate[:, columns]
            out_ref[:, columns] = value.astype(BF16)


def whole_block(shape):
    return pl.BlockSpec(shape, lambda *_: (0,) * len(shape))


def compute(
    latents, condition, context, context_cond, shift_weight, scale_weight, out_gate_weight,
    pre_gain, post_gain, query_weight, key_weight, value_weight, head_gate_weight,
    lambdas, head_gain, out_weight,
):
    params = pltpu.CompilerParams(vmem_limit_bytes=VMEM_LIMIT)
    both_axes = ("sp", "tp")
    t = lax.axis_index("tp")
    core = lax.axis_index("dp") % 2
    rows = lax.all_gather(latents[0], "tp", axis=0, tiled=False)
    other_context = lax.ppermute(
        context[0], "tp", [(i, (i + GROUP) % TP) for i in range(TP)]
    )
    partials = pl.pallas_call(
        partial_sums_kernel,
        out_shape=jax.ShapeDtypeStruct((SP * TP, 1, CHUNK), F32),
        compiler_params=params,
        name="partial_sums",
    )(condition, context_cond[None, :], shift_weight, scale_weight, out_gate_weight)
    pieces = lax.all_to_all(partials, both_axes, split_axis=0, concat_axis=0, tiled=True)
    own_sums = jnp.sum(pieces, axis=0, keepdims=True)
    copies = jnp.broadcast_to(own_sums, pieces.shape)
    sums = lax.all_to_all(copies, both_axes, split_axis=0, concat_axis=0, tiled=True)
    half = lax.dynamic_slice_in_dim(out_weight, core * GROUP * HV, GROUP * HV, 0)
    half = half + (own_sums[0, 0, 0] * 0.0).astype(BF16)
    own_half = lax.all_gather(half, "tp", axis=0, tiled=False)
    other_half = lax.ppermute(own_half, "dp", [(i, i ^ 1) for i in range(8)])
    place = jnp.stack([t % GROUP, t // GROUP]).astype(jnp.int32)
    queries, head_gate, key_values = pl.pallas_call(
        project_kernel,
        grid_spec=pltpu.PrefetchScalarGridSpec(
            num_scalar_prefetch=1,
            grid=(TP // 2,),
            in_specs=[
                pl.BlockSpec((2, ROWS, D), lambda i, _: (i, 0, 0)),
                whole_block((CTX_ROWS, D)),
                whole_block((CTX_ROWS, D)),
                whole_block((SP * TP, 1, CHUNK)),
                whole_block((1, D)),
                whole_block((D, HV)),
                whole_block((D, HV)),
                pl.BlockSpec((D, HV), lambda i, place_ref: (0, place_ref[1])),
                pl.BlockSpec((D, HV), lambda i, place_ref: (0, place_ref[1])),
            ],
            out_specs=[
                whole_block((GROUP, TP * ROWS, HV)),
                whole_block((TP * ROWS, HV)),
                whole_block((QUARTER, 2 * HV)),
            ],
            scratch_shapes=[pltpu.VMEM((TP * ROWS, D), BF16)],
        ),
        out_shape=[
            jax.ShapeDtypeStruct((GROUP, TP * ROWS, HV), BF16),
            jax.ShapeDtypeStruct((TP * ROWS, HV), BF16),
            jax.ShapeDtypeStruct((QUARTER, 2 * HV), BF16),
        ],
        compiler_params=params,
        name="project",
    )(
        place, rows, context[0], other_context, sums, pre_gain[None, :],
        query_weight, head_gate_weight, key_weight, value_weight,
    )
    key_values = lax.all_gather(key_values, "sp", axis=0, tiled=True)
    queries = lax.all_to_all(
        queries, "tp", split_axis=0, concat_axis=0, axis_index_groups=TP_GROUPS, tiled=True
    )
    peers = 4
    parts = pl.pallas_call(
        attention_kernel,
        grid=(TP // peers,),
        in_specs=[
            pl.BlockSpec(memory_space=pltpu.SMEM),
            pl.BlockSpec((GROUP, peers * ROWS, HV), lambda i: (0, i, 0)),
            whole_block((KEYS, 2 * HV)),
            pl.BlockSpec((peers * ROWS, HV), lambda i: (i, 0)),
        ],
        out_specs=pl.BlockSpec((peers, MESSAGE, HV), lambda i: (i, 0, 0)),
        out_shape=jax.ShapeDtypeStruct((TP, MESSAGE, HV), BF16),
        compiler_params=params,
        name="attention",
    )(lambdas, queries, key_values, head_gate)
    parts = lax.all_to_all(parts, "tp", split_axis=0, concat_axis=0, tiled=True)
    weight_block = pl.BlockSpec((2, GROUP * HV, D // TP), lambda i, _: (i, 0, 0))
    mixed_out = pl.pallas_call(
        finish_kernel,
        grid_spec=pltpu.PrefetchScalarGridSpec(
            num_scalar_prefetch=1,
            grid=(TP // 2,),
            in_specs=[
                whole_block((TP, MESSAGE, HV)),
                weight_block,
                weight_block,
                whole_block((SP * TP, 1, CHUNK)),
                whole_block((1, D)),
                whole_block((1, HV)),
            ],
            out_specs=whole_block((ROWS, D)),
            scratch_shapes=[
                pltpu.VMEM((2, ROWS, GROUP * HV), BF16),
                pltpu.VMEM((TP, ROWS, D // TP), F32),
            ],
        ),
        out_shape=jax.ShapeDtypeStruct((ROWS, D), BF16),
        compiler_params=params,
        name="finish",
    )(
        core.astype(jnp.int32)[None], parts, own_half, other_half, sums,
        post_gain[None, :], head_gain[None, :],
    )
    return mixed_out[None]


def solution(mesh):
    tokens = P("dp", ("sp", "tp"), None)
    channels = P(("sp", "tp"), None)
    return jax.shard_map(
        compute,
        mesh=mesh,
        in_specs=(
            tokens, P("dp", ("sp", "tp")), tokens, P(("sp", "tp")), channels, channels, channels,
            P(), P(), P(None, "tp"), P(), P(), P(None, "tp"), P("tp"), P(), P(None, "tp"),
        ),
        out_specs=tokens,
        check_vma=False,
    )
```

time: 270 us -> 246 us (0.911)
  blocking collectives: 102 us -> 63.2 us
  starting transfers between devices: 10.5 us -> 39 us
  waiting for transfers between devices: 103 us -> 93.2 us
    all_to_all x1 -> x0, blocking collectives: 37 us -> none  [summed(): lax.all_to_all(partials, axes, split_axis=0, concat_axis=0, tiled=True)]
    all_to_all x1 -> x2, starting transfers between devices: 5.94 us -> 27.9 us  [the longest x1 22 us: compute(): lax.all_to_all(partials, both_axes, split_axis=0, concat_axis=0, tiled=True)]
    all_gather x3 -> x2, waiting for transfers between devices: 88.7 us -> 73.5 us  [the longest x1 39.1 us: compute(): rows = lax.all_gather(latents[0], 'tp', axis=0, tiled=False)]
    ppermute x0 -> x2, starting transfers between devices: none -> 6.88 us  [the longest x1 4.97 us: compute(): lax.ppermute(context[0], 'tp', [(i, (i + GROUP) % TP) for i in range(TP)])]
    ppermute x0 -> x2, waiting for transfers between devices: none -> 4.08 us  [the longest x1 4.07 us: compute(): lax.ppermute(context[0], 'tp', [(i, (i + GROUP) % TP) for i in range(TP)])]
    all_to_all x1 -> x2, waiting for transfers between devices: 14.6 us -> 14.9 us  [the longest x1 14.9 us: compute(): lax.all_to_all(partials, both_axes, split_axis=0, concat_axis=0, tiled=True)]
  transfers between devices with their start and end apart: 5 -> 7, of which waited for: 3 -> 4; matrix products, arithmetic and copies ran while one was open for 1% -> 1% of each run, Pallas kernels for 8% -> 8%
where the time goes in v3:
time: 246 us; the launch traced here: 245 us
  waiting for transfers between devices  93.2 us (38%)
  blocking collectives  63.2 us (26%)
  starting transfers between devices  39 us (16%)
  Pallas kernels  29.6 us (12%)
  between operations  14.8 us (6%)
  local copies, waits for them, and re-layouts  2.89 us (1%)
  other arithmetic  2.5 us (1%)
    all_gather x1, waiting for transfers between devices, compute(): rows = lax.all_gather(latents[0], 'tp', axis=0, tiled=False)  39.1 us
    all_gather x1, waiting for transfers between devices, compute(): own_half = lax.all_gather(half, 'tp', axis=0, tiled=False)  34.3 us
    all_to_all x1, blocking collectives, compute(): parts = lax.all_to_all(parts, 'tp', split_axis=0, concat_axis=0, tiled=True)  31.8 us
    all_gather x1, blocking collectives, compute(): key_values = lax.all_gather(key_values, 'sp', axis=0, tiled=True)  31.5 us
    all_to_all x1, starting transfers between devices, compute(): lax.all_to_all(partials, both_axes, split_axis=0, concat_axis=0, tiled=True)  22 us
    all_to_all x1, waiting for transfers between devices, compute(): lax.all_to_all(partials, both_axes, split_axis=0, concat_axis=0, tiled=True)  14.9 us
    pallas_call x1, Pallas kernels, compute(): pl.pallas_call(attention_kernel, grid=(TP // peers,), in_specs=[pl.BlockS...  12.4 us
    pallas_call x1, Pallas kernels, compute(): pl.pallas_call(project_kernel, grid_spec=pltpu.PrefetchScalarGridSpec(num...  7.95 us
  transfers between devices with their start and end apart: 7, of which 4 were waited for; matrix products, arithmetic and copies ran while one was open for 1% of the time, Pallas kernels for 8%

profile of v3, /device:TPU:2, one launch (start us, length us, event | category | flops | bytes accessed | tf_op | source)
XLA Modules:
  0.0 245.2 jit_solution(11377810420595058143)
XLA Ops:
  6.5 0.0 copy-start.2
  6.5 2.0 partial_sums.1
  8.6 22.0 %all-to-all-start = ((f32[96,1,256]{2,1,0:T(1,128)}), f32[96,1,256]{2,1,0:T(1,128)S(1)}, u32[]{:S(2)}, u32[]{:S(2)}) async-start(f32[96,1,256]{2,1,0:T(1,128)} %partial_sums.1), calls=%async_computation | async-start | bytes 196608 | tf_op jit(solution)/shard_map/all_to_all | solution.py:261
  30.6 0.0 all-gather.6.cloned.1.call-start
  30.6 14.9 %all-to-all-done = f32[96,1,256]{2,1,0:T(1,128)S(1)} async-done(((f32[96,1,256]{2,1,0:T(1,128)}), f32[96,1,256]{2,1,0:T(1,128)S(1)}, u32[]{:S(2)}, u32[]{:S(2)}) %all-to-all-start) | async-done | bytes 98336 | tf_op jit(solution)/shard_map/all_to_all | solution.py:261
  45.6 0.1 reduce_sum.9
  45.7 0.5 slice.4
  46.9 1.8 dynamic-slice_add_fusion
  48.7 0.0 all-gather.6.cloned.1.call-update
  48.7 0.0 all-gather.4.cloned.1.call-start
  48.7 0.7 all-gather.4.cloned.1.call-update
  49.4 0.7 broadcast_in_dim.28
  50.1 5.9 %all-to-all-start.1 = ((f32[96,1,256]{2,1,0:T(1,128)}), f32[96,1,256]{2,1,0:T(1,128)S(1)}, u32[]{:S(2)}, u32[]{:S(2)}) async-start(f32[96,1,256]{2,1,0:T(1,128)} %broadcast_in_dim.28), calls=%async_computation.1 | async-start | bytes 196608 | tf_op jit(solution)/shard_map/all_to_all | solution.py:264
  56.1 34.3 %all-gather.6.cloned.1.call-done = bf16[4096,384]{1,0:T(8,128)(2,1)} async-done(((bf16[512,384]{1,0:T(8,128)(2,1)}), bf16[4096,384]{1,0:T(8,128)(2,1)}) %all-gather.6.cloned.1.call-update) | async-done | bytes 3145744 | tf_op jit(solution)/shard_map/all_gather | solution.py:267
  90.4 1.9 collective-permute-start.1
  92.3 0.0 copy-done.2
  92.3 5.0 %collective-permute-start = (bf16[4,3072]{1,0:T(4,128)(2,1)S(1)}, bf16[4,3072]{1,0:T(4,128)(2,1)S(1)}, u32[]{:S(2)}, u32[]{:S(2)}) collective-permute-start(bf16[4,3072]{1,0:T(4,128)(2,1)S(1)} %bitcast.15), channel_id=1, source_target_pairs={{0,32},{8,40},{16,48},{24,56},{32,0},{40,8},{48,16},{56,24},{1,33}... | collective-permute-start | bytes 73736 | tf_op jit(solution)/shard_map/ppermute | solution.py:252
  97.3 0.6 pad_add_fusion.place_ref
  97.9 4.1 %collective-permute-done.other_ref = bf16[4,3072]{1,0:T(4,128)(2,1)S(1)} collective-permute-done((bf16[4,3072]{1,0:T(4,128)(2,1)S(1)}, bf16[4,3072]{1,0:T(4,128)(2,1)S(1)}, u32[]{:S(2)}, u32[]{:S(2)}) %collective-permute-start) | collective-permute-done | bytes 24608 | tf_op jit(solution)/shard_map/ppermute | solution.py:252
  102.0 0.0 copy-start.3
  102.0 0.0 all-to-all-done.1.sums_ref
  102.0 0.0 copy-start.1
  102.0 39.1 %all-gather.4.cloned.1.call-done.rows_ref = bf16[8,64,3072]{2,1,0:T(8,128)(2,1)} async-done(((bf16[1,64,3072]{2,1,0:T(8,128)(2,1)}), bf16[8,64,3072]{2,1,0:T(8,128)(2,1)}) %all-gather.4.cloned.1.call-update) | async-done | bytes 3145744 | tf_op jit(solution)/shard_map/all_gather | solution.py:251
  141.1 0.0 copy-done.3
  141.1 0.0 copy-done.1
  141.1 8.0 %project.1 = (bf16[4,512,128]{2,1,0:T(8,128)(2,1)}, bf16[512,128]{1,0:T(8,128)(2,1)}, bf16[136,256]{1,0:T(8,128)(2,1)}) custom-call(s32[2]{0:T(128)} %pad_add_fusion.place_ref, bf16[8,64,3072]{2,1,0:T(8,128)(2,1)} %all-gather.4.cloned.1.call-done.rows_ref, bf16[4,3072]{1,0:T(4,128)(2,1)} %bitcast.14, bf16[4,3072]{1,0:T(4,128)(2,1)} %copy-done.3, ...), custom_call_target="tpu_custom_call" | custom-call | tf_op jit(solution)/shard_map/project/pallas_call | solution.py:270
  149.1 4.2 %all-to-all-start.2 = ((bf16[4,512,128]{2,1,0:T(8,128)(2,1)}), bf16[4,512,128]{2,1,0:T(8,128)(2,1)}, u32[]{:S(2)}, u32[]{:S(2)}) async-start(bf16[4,512,128]{2,1,0:T(8,128)(2,1)} %get-tuple-element.8), calls=%async_computation.2 | async-start | bytes 1048576 | tf_op jit(solution)/shard_map/all_to_all | solution.py:305
  153.9 31.5 %all_gather.13.kv_ref = bf16[1632,256]{1,0:T(8,128)(2,1)} all-gather(bf16[136,256]{1,0:T(8,128)(2,1)} %get-tuple-element.9), channel_id=1, replica_groups=mesh['sp'=12,'tp'=8,'dp'=8] {'sp'}, dimensions={0}, use_global_device_ids=true | all-gather | bytes 905216 | tf_op jit(solution)/shard_map/all_gather | solution.py:304
  185.4 0.0 all-to-all-done.2.q_ref
  185.4 12.4 %attention.1 = bf16[8,592,128]{2,1,0:T(8,128)(2,1)} custom-call(f32[1]{0:T(128)S(6)} %copy.17.lambda_ref, bf16[4,512,128]{2,1,0:T(8,128)(2,1)} %all-to-all-done.2.q_ref, bf16[1632,256]{1,0:T(8,128)(2,1)} %all_gather.13.kv_ref, bf16[512,128]{1,0:T(8,128)(2,1)} %get-tuple-element.10.gate_ref), custom_call_target="tpu_custom_call" | custom-call | tf_op jit(solution)/shard_map/attention/pallas_call | solution.py:309
  197.8 31.8 %all_to_all.20.parts_ref = bf16[8,592,128]{2,1,0:T(8,128)(2,1)} all-to-all(bf16[8,592,128]{2,1,0:T(8,128)(2,1)} %attention.1), channel_id=1, replica_groups=mesh['sp'=12,'tp'=8,'dp'=8] {'tp'}, dimensions={0} | all-to-all | bytes 2424832 | tf_op jit(solution)/shard_map/all_to_all | solution.py:323
  229.5 0.0 collective-permute-done.1.other_ref
  229.5 0.0 copy-start
  229.5 1.7 copy-done
  231.2 7.2 %finish.1 = bf16[64,3072]{1,0:T(8,128)(2,1)} custom-call(s32[1]{0:T(128)} %bitcast.core_ref, bf16[8,592,128]{2,1,0:T(8,128)(2,1)} %all_to_all.20.parts_ref, bf16[8,512,384]{2,1,0:T(8,128)(2,1)} %bitcast.13, bf16[8,512,384]{2,1,0:T(8,128)(2,1)} %copy-done, f32[96,1,256]{2,1,0:T(1,128)} %copy-done.1, f32[1,3072]{1,0:T(1,128)} %bitcast.17, f32[1,128]{1,0:T(1,128)} %bitcast.19), custom_call_target="tpu_custom_call" | custom-call | tf_op jit(solution)/shard_map/finish/pallas_call | solution.py:325
Async XLA Ops:
  6.5 85.8 %copy-start.2 = (bf16[1,4,3072]{2,1,0:T(4,128)(2,1)S(1)}, bf16[1,4,3072]{2,1,0:T(4,128)(2,1)}, u32[]{:S(2)}) copy-start(bf16[1,4,3072]{2,1,0:T(4,128)(2,1)} %param.18) | copy-start | bytes 73732
  8.6 37.0 %all-to-all-start = ((f32[96,1,256]{2,1,0:T(1,128)}), f32[96,1,256]{2,1,0:T(1,128)S(1)}, u32[]{:S(2)}, u32[]{:S(2)}) async-start(f32[96,1,256]{2,1,0:T(1,128)} %partial_sums.1), calls=%async_computation | async-start | bytes 196608 | tf_op jit(solution)/shard_map/all_to_all | solution.py:261
  30.6 59.8 %all-gather.6.cloned.1.call-start = ((), (), s32[]{:S(2)}) async-start(), calls=%async_computation.5 | async-start | bytes 3538944 | tf_op jit(solution)/shard_map/all_gather | solution.py:267
  48.7 92.4 %all-gather.4.cloned.1.call-start = ((), (), s32[]{:S(2)}) async-start(), calls=%async_computation.4 | async-start | bytes 3538944 | tf_op jit(solution)/shard_map/all_gather | solution.py:251
  50.1 51.8 %all-to-all-start.1 = ((f32[96,1,256]{2,1,0:T(1,128)}), f32[96,1,256]{2,1,0:T(1,128)S(1)}, u32[]{:S(2)}, u32[]{:S(2)}) async-start(f32[96,1,256]{2,1,0:T(1,128)} %broadcast_in_dim.28), calls=%async_computation.1 | async-start | bytes 196608 | tf_op jit(solution)/shard_map/all_to_all | solution.py:264
  90.4 139.1 %collective-permute-start.1 = (bf16[8,512,384]{2,1,0:T(8,128)(2,1)}, bf16[8,512,384]{2,1,0:T(8,128)(2,1)S(1)}, u32[]{:S(2)}, u32[]{:S(2)}) collective-permute-start(bf16[8,512,384]{2,1,0:T(8,128)(2,1)} %bitcast.12), channel_id=1, source_target_pairs={{0,1},{1,0},{2,3},{3,2},{4,5},{5,4},{6,7},{7,6},{8,9},{9,8},{10,11... | collective-permute-start | bytes 9437192 | tf_op jit(solution)/shard_map/ppermute | solution.py:268
  92.3 9.6 %collective-permute-start = (bf16[4,3072]{1,0:T(4,128)(2,1)S(1)}, bf16[4,3072]{1,0:T(4,128)(2,1)S(1)}, u32[]{:S(2)}, u32[]{:S(2)}) collective-permute-start(bf16[4,3072]{1,0:T(4,128)(2,1)S(1)} %bitcast.15), channel_id=1, source_target_pairs={{0,32},{8,40},{16,48},{24,56},{32,0},{40,8},{48,16},{56,24},{1,33}... | collective-permute-start | bytes 73736 | tf_op jit(solution)/shard_map/ppermute | solution.py:252
  102.0 39.2 %copy-start.3 = (bf16[4,3072]{1,0:T(4,128)(2,1)}, bf16[4,3072]{1,0:T(4,128)(2,1)S(1)}, u32[]{:S(2)}) copy-start(bf16[4,3072]{1,0:T(4,128)(2,1)S(1)} %collective-permute-done.other_ref) | copy-start | bytes 73732
  102.0 39.2 %copy-start.1 = (f32[96,1,256]{2,1,0:T(1,128)}, f32[96,1,256]{2,1,0:T(1,128)S(1)}, u32[]{:S(2)}) copy-start(f32[96,1,256]{2,1,0:T(1,128)S(1)} %all-to-all-done.1.sums_ref) | copy-start | bytes 294916
  149.1 36.3 %all-to-all-start.2 = ((bf16[4,512,128]{2,1,0:T(8,128)(2,1)}), bf16[4,512,128]{2,1,0:T(8,128)(2,1)}, u32[]{:S(2)}, u32[]{:S(2)}) async-start(bf16[4,512,128]{2,1,0:T(8,128)(2,1)} %get-tuple-element.8), calls=%async_computation.2 | async-start | bytes 1048576 | tf_op jit(solution)/shard_map/all_to_all | solution.py:305
  229.5 1.7 copy-start
Sparse Core Ops, SparseCore 0:
  48.8 41.5 all-gather.5
  92.8 48.2 all-gather.3

commit v4 on v3

--- a/solution.py
+++ b/solution.py
@@ -22,12 +22,15 @@
 MESSAGE = STAT_ROW + 2 * STATS
 CHUNK = 256
 CHAIN = 512
+FINISH_PIECES = 4
+PROJECT_PIECES = 4
 VECTOR_ROWS = D // CHUNK
 SCALE = HQK ** (-0.5) * 1.4426950408889634
 NORM_EPSILON = 1e-06
 F32 = jnp.float32
 BF16 = jnp.bfloat16
 TP_GROUPS = [[0, 1, 2, 3], [4, 5, 6, 7]]
+CORE_PAIRS = [[0, 1], [2, 3], [4, 5], [6, 7]]
 VMEM_LIMIT = 60 * 1024 * 1024
 
 
@@ -69,29 +72,28 @@
 ):
     step = pl.program_id(0)
     pieces = rows_ref.shape[0]
+    block = pieces * ROWS
     gain = gain_ref[...]
     scale, shift = gain * (1.0 + vector_of(sums_ref, 1)), vector_of(sums_ref, 0)
-    for piece in range(pieces):
-        first = pl.multiple_of((step * pieces + piece) * ROWS, ROWS)
-        latent_ref[pl.ds(first, ROWS), :] = modulated(rows_ref[piece], scale, shift)
-
-    @pl.when(step == pl.num_programs(0) - 1)
+    latent = modulated(rows_ref[...].reshape(block, D), scale, shift)
+    weight = jnp.concatenate([query_weight_ref[...], gate_weight_ref[...]], axis=1)
+    projected = jnp.dot(latent, weight, preferred_element_type=F32).astype(BF16)
+    first = pl.multiple_of(step * block, block)
+    for copy in range(GROUP):
+        q_ref[copy, pl.ds(first, block), :] = projected[:, :HV]
+    gate_ref[pl.ds(first, block), :] = projected[:, HV:]
+    quarter_step = place_ref[0] * 2 // pieces
+
+    @pl.when(step == quarter_step)
     def _():
-        weight = jnp.concatenate([query_weight_ref[...], gate_weight_ref[...]], axis=1)
-        projected = jnp.dot(latent_ref[...], weight, preferred_element_type=F32)
-        queries = projected[:, :HV].astype(BF16)
-        for copy in range(GROUP):
-            q_ref[copy] = queries
-        gate_ref[...] = projected[:, HV:].astype(BF16)
         weight = jnp.concatenate([key_weight_ref[...], value_weight_ref[...]], axis=1)
-        first = pl.multiple_of(place_ref[0] * 2 * ROWS, 2 * ROWS)
-        kv = jnp.dot(latent_ref[pl.ds(first, 2 * ROWS), :], weight, preferred_element_type=F32)
-        kv_ref[: 2 * ROWS, :] = kv.astype(BF16)
         context = jnp.concatenate([own_ref[...].astype(F32), other_ref[...].astype(F32)], axis=0)
         context_scale = gain * (1.0 + vector_of(sums_ref, 4))
         context = modulated(context, context_scale, vector_of(sums_ref, 3))
-        kv = jnp.dot(context, weight, preferred_element_type=F32)
-        kv_ref[2 * ROWS :, :] = kv.astype(BF16)
+        latent_ref[...] = latent
+        inner = pl.multiple_of((place_ref[0] * 2 - quarter_step * pieces) * ROWS, 2 * ROWS)
+        tokens = jnp.concatenate([latent_ref[pl.ds(inner, 2 * ROWS), :], context], axis=0)
+        kv_ref[...] = jnp.dot(tokens, weight, preferred_element_type=F32).astype(BF16)
 
 
 def three_parts(value):
@@ -167,8 +169,7 @@
 
 
 def finish_kernel(
-    core_ref, parts_ref, own_ref, other_ref, sums_ref, post_gain_ref, head_gain_ref,
-    out_ref, branch_ref, projected_ref,
+    parts_ref, weight_ref, sums_ref, post_gain_ref, head_gain_ref, out_ref, branch_ref, projected_ref
 ):
     step = pl.program_id(0)
 
@@ -209,15 +210,12 @@
             square = jnp.mean(attended * attended, axis=-1, keepdims=True)
             gate = parts_ref[head, GATE_ROW:STAT_ROW, :].astype(F32)
             branch = attended * lax.rsqrt(square + NORM_EPSILON) * head_gain_ref[...] * silu(gate)
-            branch_ref[g, :, j * HV : (j + 1) * HV] = branch.astype(BF16)
-
-    own = core_ref[0]
-    pieces = own_ref.shape[0]
+            branch_ref[:, head * HV : (head + 1) * HV] = branch.astype(BF16)
+
+    pieces = weight_ref.shape[1]
     for piece in range(pieces):
-        projected = jnp.dot(branch_ref[own], own_ref[piece], preferred_element_type=F32)
-        projected = projected + jnp.dot(
-            branch_ref[1 - own], other_ref[piece], preferred_element_type=F32
-        )
+        weight = weight_ref[:, piece].reshape(TP * HV, D // TP)
+        projected = jnp.dot(branch_ref[...], weight, preferred_element_type=F32)
         projected_ref[step * pieces + piece] = projected.astype(BF16).astype(F32)
 
     @pl.when(step == pl.num_programs(0) - 1)
@@ -264,16 +262,16 @@
     sums = lax.all_to_all(copies, both_axes, split_axis=0, concat_axis=0, tiled=True)
     half = lax.dynamic_slice_in_dim(out_weight, core * GROUP * HV, GROUP * HV, 0)
     half = half + (own_sums[0, 0, 0] * 0.0).astype(BF16)
-    own_half = lax.all_gather(half, "tp", axis=0, tiled=False)
-    other_half = lax.ppermute(own_half, "dp", [(i, i ^ 1) for i in range(8)])
+    halves = lax.all_gather(half, "tp", axis=0, tiled=False)
+    out_weights = lax.all_gather(halves, "dp", axis=0, tiled=False, axis_index_groups=CORE_PAIRS)
     place = jnp.stack([t % GROUP, t // GROUP]).astype(jnp.int32)
     queries, head_gate, key_values = pl.pallas_call(
         project_kernel,
         grid_spec=pltpu.PrefetchScalarGridSpec(
             num_scalar_prefetch=1,
-            grid=(TP // 2,),
+            grid=(TP // PROJECT_PIECES,),
             in_specs=[
-                pl.BlockSpec((2, ROWS, D), lambda i, _: (i, 0, 0)),
+                pl.BlockSpec((PROJECT_PIECES, ROWS, D), lambda i, _: (i, 0, 0)),
                 whole_block((CTX_ROWS, D)),
                 whole_block((CTX_ROWS, D)),
                 whole_block((SP * TP, 1, CHUNK)),
@@ -288,7 +286,7 @@
                 whole_block((TP * ROWS, HV)),
                 whole_block((QUARTER, 2 * HV)),
             ],
-            scratch_shapes=[pltpu.VMEM((TP * ROWS, D), BF16)],
+            scratch_shapes=[pltpu.VMEM((PROJECT_PIECES * ROWS, D), BF16)],
         ),
         out_shape=[
             jax.ShapeDtypeStruct((GROUP, TP * ROWS, HV), BF16),
@@ -321,33 +319,22 @@
         name="attention",
     )(lambdas, queries, key_values, head_gate)
     parts = lax.all_to_all(parts, "tp", split_axis=0, concat_axis=0, tiled=True)
-    weight_block = pl.BlockSpec((2, GROUP * HV, D // TP), lambda i, _: (i, 0, 0))
     mixed_out = pl.pallas_call(
         finish_kernel,
-        grid_spec=pltpu.PrefetchScalarGridSpec(
-            num_scalar_prefetch=1,
-            grid=(TP // 2,),
-            in_specs=[
-                whole_block((TP, MESSAGE, HV)),
-                weight_block,
-                weight_block,
-                whole_block((SP * TP, 1, CHUNK)),
-                whole_block((1, D)),
-                whole_block((1, HV)),
-            ],
-            out_specs=whole_block((ROWS, D)),
-            scratch_shapes=[
-                pltpu.VMEM((2, ROWS, GROUP * HV), BF16),
-                pltpu.VMEM((TP, ROWS, D // TP), F32),
-            ],
-        ),
+        grid=(TP // FINISH_PIECES,),
+        in_specs=[
+            whole_block((TP, MESSAGE, HV)),
+            pl.BlockSpec((2, FINISH_PIECES, GROUP * HV, D // TP), lambda i: (0, i, 0, 0)),
+            whole_block((SP * TP, 1, CHUNK)),
+            whole_block((1, D)),
+            whole_block((1, HV)),
+        ],
+        out_specs=whole_block((ROWS, D)),
         out_shape=jax.ShapeDtypeStruct((ROWS, D), BF16),
+        scratch_shapes=[pltpu.VMEM((ROWS, TP * HV), BF16), pltpu.VMEM((TP, ROWS, D // TP), F32)],
         compiler_params=params,
         name="finish",
-    )(
-        core.astype(jnp.int32)[None], parts, own_half, other_half, sums,
-        post_gain[None, :], head_gain[None, :],
-    )
+    )(parts, out_weights, sums, post_gain[None, :], head_gain[None, :])
     return mixed_out[None]
 
 

time: 246 us -> 242 us (0.984)
  the two profiles are of different devices: /device:TPU:2 before, /device:TPU:4 now
where the time goes in v4:
time: 242 us
  waiting for transfers between devices  85.7 us (35%)
  blocking collectives  62.3 us (26%)
  starting transfers between devices  47.5 us (20%)
  Pallas kernels  27.1 us (11%)
  between operations  14.5 us (6%)
  other arithmetic  2.53 us (1%)
    all_gather x1, waiting for transfers between devices, compute(): halves = lax.all_gather(half, 'tp', axis=0, tiled=False)  38.9 us
    all_to_all x1, blocking collectives, compute(): parts = lax.all_to_all(parts, 'tp', split_axis=0, concat_axis=0, tiled=True)  32.1 us
    all_gather x1, blocking collectives, compute(): key_values = lax.all_gather(key_values, 'sp', axis=0, tiled=True)  30.3 us
    all_gather x1, waiting for transfers between devices, compute(): rows = lax.all_gather(latents[0], 'tp', axis=0, tiled=False)  24.4 us
    all_to_all x1, starting transfers between devices, compute(): lax.all_to_all(partials, both_axes, split_axis=0, concat_axis=0, tiled=True)  22 us
    all_to_all x1, waiting for transfers between devices, compute(): lax.all_to_all(partials, both_axes, split_axis=0, concat_axis=0, tiled=True)  14.9 us
    all_to_all x1, starting transfers between devices, compute(): lax.all_to_all(copies, both_axes, split_axis=0, concat_axis=0, tiled=True)  14.3 us
    pallas_call x1, Pallas kernels, compute(): pl.pallas_call(attention_kernel, grid=(TP // peers,), in_specs=[pl.BlockS...  12.4 us
  transfers between devices with their start and end apart: 7, of which 5 were waited for; matrix products, arithmetic and copies ran while one was open for 1% of the time, Pallas kernels for 8%

profile of v4, /device:TPU:4, one launch (start us, length us, event | category | flops | bytes accessed | tf_op | source)
XLA Modules:
  0.0 241.7 jit_solution(7200191696475780091)
XLA Ops:
  6.5 2.0 partial_sums.1
  8.6 22.0 %all-to-all-start = ((f32[96,1,256]{2,1,0:T(1,128)}), f32[96,1,256]{2,1,0:T(1,128)S(1)}, u32[]{:S(2)}, u32[]{:S(2)}) async-start(f32[96,1,256]{2,1,0:T(1,128)} %partial_sums.1), calls=%async_computation | async-start | bytes 196608 | tf_op jit(solution)/shard_map/all_to_all | solution.py:259
  30.6 0.0 all-gather.8.cloned.1.call-start
  30.6 14.9 %all-to-all-done = f32[96,1,256]{2,1,0:T(1,128)S(1)} async-done(((f32[96,1,256]{2,1,0:T(1,128)}), f32[96,1,256]{2,1,0:T(1,128)S(1)}, u32[]{:S(2)}, u32[]{:S(2)}) %all-to-all-start) | async-done | bytes 98336 | tf_op jit(solution)/shard_map/all_to_all | solution.py:259
  45.6 0.1 reduce_sum.9
  45.7 0.5 slice.4
  46.8 1.8 dynamic-slice_add_fusion
  48.7 0.0 all-gather.8.cloned.1.call-update
  48.7 0.0 all-gather.6.cloned.1.call-start
  48.7 0.7 all-gather.6.cloned.1.call-update
  49.4 0.0 all-gather.10.cloned.1.call-start
  49.5 38.9 %all-gather.8.cloned.1.call-done = bf16[4096,384]{1,0:T(8,128)(2,1)} async-done(((bf16[512,384]{1,0:T(8,128)(2,1)}), bf16[4096,384]{1,0:T(8,128)(2,1)}) %all-gather.8.cloned.1.call-update) | async-done | bytes 3145744 | tf_op jit(solution)/shard_map/all_gather | solution.py:265
  88.4 0.0 copy-start.2
  88.4 0.0 all-gather.10.cloned.1.call-update
  88.5 0.7 broadcast_in_dim.24
  89.1 14.3 %all-to-all-start.1 = ((f32[96,1,256]{2,1,0:T(1,128)}), f32[96,1,256]{2,1,0:T(1,128)S(1)}, u32[]{:S(2)}, u32[]{:S(2)}) async-start(f32[96,1,256]{2,1,0:T(1,128)} %broadcast_in_dim.24), calls=%async_computation.1 | async-start | bytes 196608 | tf_op jit(solution)/shard_map/all_to_all | solution.py:262
  103.4 0.0 copy-done.2
  103.4 7.2 %collective-permute-start = (bf16[4,3072]{1,0:T(4,128)(2,1)S(1)}, bf16[4,3072]{1,0:T(4,128)(2,1)S(1)}, u32[]{:S(2)}, u32[]{:S(2)}) collective-permute-start(bf16[4,3072]{1,0:T(4,128)(2,1)S(1)} %bitcast.15), channel_id=1, source_target_pairs={{0,32},{8,40},{16,48},{24,56},{32,0},{40,8},{48,16},{56,24},{1,33}... | collective-permute-start | bytes 73736 | tf_op jit(solution)/shard_map/ppermute | solution.py:250
  110.6 0.6 pad_add_fusion.place_ref
  111.2 2.7 %collective-permute-done.other_ref = bf16[4,3072]{1,0:T(4,128)(2,1)S(1)} collective-permute-done((bf16[4,3072]{1,0:T(4,128)(2,1)S(1)}, bf16[4,3072]{1,0:T(4,128)(2,1)S(1)}, u32[]{:S(2)}, u32[]{:S(2)}) %collective-permute-start) | collective-permute-done | bytes 24608 | tf_op jit(solution)/shard_map/ppermute | solution.py:250
  113.9 0.0 copy-start.3
  113.9 4.1 %all-to-all-done.1.sums_ref = f32[96,1,256]{2,1,0:T(1,128)S(1)} async-done(((f32[96,1,256]{2,1,0:T(1,128)}), f32[96,1,256]{2,1,0:T(1,128)S(1)}, u32[]{:S(2)}, u32[]{:S(2)}) %all-to-all-start.1) | async-done | bytes 98336 | tf_op jit(solution)/shard_map/all_to_all | solution.py:262
  118.0 0.0 copy-start.1
  118.0 24.4 %all-gather.6.cloned.1.call-done.rows_ref = bf16[8,64,3072]{2,1,0:T(8,128)(2,1)} async-done(((bf16[1,64,3072]{2,1,0:T(8,128)(2,1)}), bf16[8,64,3072]{2,1,0:T(8,128)(2,1)}) %all-gather.6.cloned.1.call-update) | async-done | bytes 3145744 | tf_op jit(solution)/shard_map/all_gather | solution.py:249
  142.3 0.0 copy-done.3
  142.3 0.0 copy-done.1
  142.3 6.4 %project.1 = (bf16[4,512,128]{2,1,0:T(8,128)(2,1)}, bf16[512,128]{1,0:T(8,128)(2,1)}, bf16[136,256]{1,0:T(8,128)(2,1)}) custom-call(s32[2]{0:T(128)} %pad_add_fusion.place_ref, bf16[8,64,3072]{2,1,0:T(8,128)(2,1)} %all-gather.6.cloned.1.call-done.rows_ref, bf16[4,3072]{1,0:T(4,128)(2,1)} %bitcast.14, bf16[4,3072]{1,0:T(4,128)(2,1)} %copy-done.3, ...), custom_call_target="tpu_custom_call" | custom-call | tf_op jit(solution)/shard_map/project/pallas_call | solution.py:268
  148.8 4.0 %all-to-all-start.2 = ((bf16[4,512,128]{2,1,0:T(8,128)(2,1)}), bf16[4,512,128]{2,1,0:T(8,128)(2,1)S(1)}, u32[]{:S(2)}, u32[]{:S(2)}) async-start(bf16[4,512,128]{2,1,0:T(8,128)(2,1)} %get-tuple-element.8), calls=%async_computation.2 | async-start | bytes 1048576 | tf_op jit(solution)/shard_map/all_to_all | solution.py:303
  153.4 30.3 %all_gather.19.kv_ref = bf16[1632,256]{1,0:T(8,128)(2,1)} all-gather(bf16[136,256]{1,0:T(8,128)(2,1)} %get-tuple-element.9), channel_id=1, replica_groups=mesh['sp'=12,'tp'=8,'dp'=8] {'sp'}, dimensions={0}, use_global_device_ids=true | all-gather | bytes 905216 | tf_op jit(solution)/shard_map/all_gather | solution.py:302
  183.7 0.0 all-to-all-done.2.q_ref
  183.7 0.0 copy-start
  183.7 0.8 copy-done
  184.5 12.4 %attention.1 = bf16[8,592,128]{2,1,0:T(8,128)(2,1)} custom-call(f32[1]{0:T(128)S(6)} %copy.17.lambda_ref, bf16[4,512,128]{2,1,0:T(8,128)(2,1)} %copy-done, bf16[1632,256]{1,0:T(8,128)(2,1)} %all_gather.19.kv_ref, bf16[512,128]{1,0:T(8,128)(2,1)} %get-tuple-element.10.gate_ref), custom_call_target="tpu_custom_call" | custom-call | tf_op jit(solution)/shard_map/attention/pallas_call | solution.py:307
  196.9 32.1 %all_to_all.20.parts_ref = bf16[8,592,128]{2,1,0:T(8,128)(2,1)} all-to-all(bf16[8,592,128]{2,1,0:T(8,128)(2,1)} %attention.1), channel_id=1, replica_groups=mesh['sp'=12,'tp'=8,'dp'=8] {'tp'}, dimensions={0} | all-to-all | bytes 2424832 | tf_op jit(solution)/shard_map/all_to_all | solution.py:321
  228.9 0.0 all-gather.10.cloned.1.call-done
  228.9 6.2 %finish.1 = bf16[64,3072]{1,0:T(8,128)(2,1)} custom-call(bf16[8,592,128]{2,1,0:T(8,128)(2,1)} %all_to_all.20.parts_ref, bf16[2,8,512,384]{3,2,1,0:T(8,128)(2,1)} %bitcast.12, f32[96,1,256]{2,1,0:T(1,128)} %copy-done.1, f32[1,3072]{1,0:T(1,128)} %bitcast.17, f32[1,128]{1,0:T(1,128)} %bitcast.19), custom_call_target="tpu_custom_call" | custom-call | tf_op jit(solution)/shard_map/finish/pallas_call | solution.py:322
Async XLA Ops:
  8.6 37.0 %all-to-all-start = ((f32[96,1,256]{2,1,0:T(1,128)}), f32[96,1,256]{2,1,0:T(1,128)S(1)}, u32[]{:S(2)}, u32[]{:S(2)}) async-start(f32[96,1,256]{2,1,0:T(1,128)} %partial_sums.1), calls=%async_computation | async-start | bytes 196608 | tf_op jit(solution)/shard_map/all_to_all | solution.py:259
  30.6 57.9 %all-gather.8.cloned.1.call-start = ((), (), s32[]{:S(2)}) async-start(), calls=%async_computation.5 | async-start | bytes 3538944 | tf_op jit(solution)/shard_map/all_gather | solution.py:265
  48.7 93.6 %all-gather.6.cloned.1.call-start = ((), (), s32[]{:S(2)}) async-start(), calls=%async_computation.4 | async-start | bytes 3538944 | tf_op jit(solution)/shard_map/all_gather | solution.py:249
  49.4 179.5 %all-gather.10.cloned.1.call-start = ((), (), s32[]{:S(2)}) async-start(), calls=%async_computation.6 | async-start | bytes 9437184 | tf_op jit(solution)/shard_map/all_gather | solution.py:266
  88.4 15.0 %copy-start.2 = (bf16[1,4,3072]{2,1,0:T(4,128)(2,1)S(1)}, bf16[1,4,3072]{2,1,0:T(4,128)(2,1)}, u32[]{:S(2)}) copy-start(bf16[1,4,3072]{2,1,0:T(4,128)(2,1)} %param.18) | copy-start | bytes 73732
  89.1 28.8 %all-to-all-start.1 = ((f32[96,1,256]{2,1,0:T(1,128)}), f32[96,1,256]{2,1,0:T(1,128)S(1)}, u32[]{:S(2)}, u32[]{:S(2)}) async-start(f32[96,1,256]{2,1,0:T(1,128)} %broadcast_in_dim.24), calls=%async_computation.1 | async-start | bytes 196608 | tf_op jit(solution)/shard_map/all_to_all | solution.py:262
  103.4 10.5 %collective-permute-start = (bf16[4,3072]{1,0:T(4,128)(2,1)S(1)}, bf16[4,3072]{1,0:T(4,128)(2,1)S(1)}, u32[]{:S(2)}, u32[]{:S(2)}) collective-permute-start(bf16[4,3072]{1,0:T(4,128)(2,1)S(1)} %bitcast.15), channel_id=1, source_target_pairs={{0,32},{8,40},{16,48},{24,56},{32,0},{40,8},{48,16},{56,24},{1,33}... | collective-permute-start | bytes 73736 | tf_op jit(solution)/shard_map/ppermute | solution.py:250
  113.9 28.4 %copy-start.3 = (bf16[4,3072]{1,0:T(4,128)(2,1)}, bf16[4,3072]{1,0:T(4,128)(2,1)S(1)}, u32[]{:S(2)}) copy-start(bf16[4,3072]{1,0:T(4,128)(2,1)S(1)} %collective-permute-done.other_ref) | copy-start | bytes 73732
  118.0 24.4 %copy-start.1 = (f32[96,1,256]{2,1,0:T(1,128)}, f32[96,1,256]{2,1,0:T(1,128)S(1)}, u32[]{:S(2)}) copy-start(f32[96,1,256]{2,1,0:T(1,128)S(1)} %all-to-all-done.1.sums_ref) | copy-start | bytes 294916
  148.8 34.9 %all-to-all-start.2 = ((bf16[4,512,128]{2,1,0:T(8,128)(2,1)}), bf16[4,512,128]{2,1,0:T(8,128)(2,1)S(1)}, u32[]{:S(2)}, u32[]{:S(2)}) async-start(bf16[4,512,128]{2,1,0:T(8,128)(2,1)} %get-tuple-element.8), calls=%async_computation.2 | async-start | bytes 1048576 | tf_op jit(solution)/shard_map/all_to_all | solution.py:303
  183.7 0.8 copy-start
Sparse Core Ops, SparseCore 0:
  48.8 39.5 all-gather.7
  90.8 51.4 all-gather.5
  144.7 25.1 all-gather.9

commit v5 on v4

--- a/solution.py
+++ b/solution.py
@@ -1,3 +1,5 @@
+import functools
+
 import jax
 import jax.numpy as jnp
 from jax import lax
@@ -16,12 +18,12 @@
 SP = 12
 QUARTER = 2 * (ROWS + CTX_ROWS)
 KEYS = SP * QUARTER
-STATS = GROUP * 2
-GATE_ROW = STATS * ROWS
-STAT_ROW = GATE_ROW + ROWS
-MESSAGE = STAT_ROW + 2 * STATS
+STATS = 8
+PARTS = GROUP
+GATE_ROW = PARTS * ROWS
 CHUNK = 256
 CHAIN = 512
+PEERS = 8
 FINISH_PIECES = 4
 PROJECT_PIECES = 4
 VECTOR_ROWS = D // CHUNK
@@ -104,14 +106,18 @@
     return high.astype(F32), middle.astype(F32), low.astype(F32)
 
 
-def attention_kernel(lambda_ref, q_ref, kv_ref, gate_ref, out_ref):
+def attention_kernel(with_gate, *refs):
+    if with_gate:
+        lambda_ref, gate_ref, q_ref, kv_ref, out_ref = refs
+    else:
+        q_ref, kv_ref, out_ref = refs
     peers = out_ref.shape[0]
     block = peers * ROWS
-    q = q_ref[...].reshape(GROUP * block, 2 * HQK)
+    q = q_ref[...].reshape(q_ref.shape[0] * block, 2 * HQK)
     keys = kv_ref[:, : 2 * HQK]
     value_rows = kv_ref[:, 2 * HQK :]
     lane = lax.broadcasted_iota(jnp.int32, (CHAIN, 2 * HQK), 1)
-    chains = [(first, m) for first in range(0, GROUP * block, CHAIN) for m in range(2)]
+    chains = [(first, m) for first in range(0, q.shape[0], CHAIN) for m in range(2)]
 
     def scores_of(first, m):
         rows = q[first : first + CHAIN]
@@ -158,18 +164,22 @@
     high, middle, low = three_parts(jnp.transpose(stats)[:STATS])
     row = lax.broadcasted_iota(jnp.int32, (STATS, ROWS), 0)
     own_lambda = jnp.zeros((STATS, ROWS), F32)
-    for part, piece in enumerate(three_parts(jnp.full((STATS, ROWS), lambda_ref[0], F32))):
-        own_lambda = jnp.where(row == part, piece, own_lambda)
+    if with_gate:
+        for part, piece in enumerate(three_parts(jnp.full((STATS, ROWS), lambda_ref[0], F32))):
+            own_lambda = jnp.where(row == part, piece, own_lambda)
+    stat_row = out_ref.shape[1] - 2 * STATS
     for p in range(peers):
         lanes = slice(p * ROWS, (p + 1) * ROWS)
-        out_ref[p, GATE_ROW:STAT_ROW, :] = gate_ref[lanes, :]
+        if with_gate:
+            out_ref[p, GATE_ROW:stat_row, :] = gate_ref[lanes, :]
         upper = jnp.concatenate([high[:, lanes], middle[:, lanes]], axis=1)
         lower = jnp.concatenate([low[:, lanes], own_lambda], axis=1)
-        out_ref[p, STAT_ROW:, :] = jnp.concatenate([upper, lower], axis=0).astype(BF16)
+        out_ref[p, stat_row:, :] = jnp.concatenate([upper, lower], axis=0).astype(BF16)
 
 
 def finish_kernel(
-    parts_ref, weight_ref, sums_ref, post_gain_ref, head_gain_ref, out_ref, branch_ref, projected_ref
+    first_ref, second_ref, weight_ref, sums_ref, post_gain_ref, head_gain_ref,
+    out_ref, branch_ref, projected_ref,
 ):
     step = pl.program_id(0)
 
@@ -177,10 +187,15 @@
     def _():
         levels, lambdas = [], []
         for t in range(TP):
-            stats = parts_ref[t, STAT_ROW:, :].astype(F32)
-            upper, lower = stats[:STATS], stats[STATS:]
-            levels.append(upper[:, :ROWS] + upper[:, ROWS:] + lower[:, :ROWS])
-            lambdas.append(lower[0:1, ROWS:] + lower[1:2, ROWS:] + lower[2:3, ROWS:])
+            both = []
+            for parts_ref in (first_ref, second_ref):
+                stats = parts_ref[t, parts_ref.shape[1] - 2 * STATS :, :].astype(F32)
+                upper, lower = stats[:STATS], stats[STATS:]
+                level = upper[:, :ROWS] + upper[:, ROWS:] + lower[:, :ROWS]
+                both.append(level[:PARTS])
+                if parts_ref is first_ref:
+                    lambdas.append(lower[0:1, ROWS:] + lower[1:2, ROWS:] + lower[2:3, ROWS:])
+            levels.append(jnp.concatenate(both, axis=0))
         shares = []
         for g in range(TP // GROUP):
             group = levels[g * GROUP : (g + 1) * GROUP]
@@ -200,15 +215,17 @@
             for m in range(2):
                 index = 2 * j + m
                 ratio = jnp.zeros((ROWS, HV), F32)
+                parts_ref = first_ref if index < PARTS else second_ref
+                first = index % PARTS * ROWS
                 for t in range(g * GROUP, (g + 1) * GROUP):
-                    part = parts_ref[t, index * ROWS : (index + 1) * ROWS, :].astype(F32)
+                    part = parts_ref[t, first : first + ROWS, :].astype(F32)
                     column = t * STATS + index
                     ratio = ratio + columns[:, column : column + 1] * part
                 ratios.append(ratio)
             column = TP * STATS + head
             attended = ratios[0] - columns[:, column : column + 1] * ratios[1]
             square = jnp.mean(attended * attended, axis=-1, keepdims=True)
-            gate = parts_ref[head, GATE_ROW:STAT_ROW, :].astype(F32)
+            gate = first_ref[head, GATE_ROW : GATE_ROW + ROWS, :].astype(F32)
             branch = attended * lax.rsqrt(square + NORM_EPSILON) * head_gain_ref[...] * silu(gate)
             branch_ref[:, head * HV : (head + 1) * HV] = branch.astype(BF16)
 
@@ -235,6 +252,26 @@
 
 def whole_block(shape):
     return pl.BlockSpec(shape, lambda *_: (0,) * len(shape))
+
+
+def attend(queries, key_values, half, params, extra):
+    rows = GATE_ROW + (ROWS if extra else 0) + 2 * STATS
+    extra_specs = [
+        pl.BlockSpec(memory_space=pltpu.SMEM), pl.BlockSpec((PEERS * ROWS, HV), lambda i: (i, 0))
+    ]
+    return pl.pallas_call(
+        functools.partial(attention_kernel, bool(extra)),
+        grid=(TP // PEERS,),
+        in_specs=(extra_specs if extra else [])
+        + [
+            pl.BlockSpec((GROUP // 2, PEERS * ROWS, HV), lambda i: (half, i, 0)),
+            whole_block((KEYS, 2 * HV)),
+        ],
+        out_specs=pl.BlockSpec((PEERS, rows, HV), lambda i: (i, 0, 0)),
+        out_shape=jax.ShapeDtypeStruct((TP, rows, HV), BF16),
+        compiler_params=params,
+        name="attention",
+    )(*extra, queries, key_values)
 
 
 def compute(
@@ -303,27 +340,16 @@
     queries = lax.all_to_all(
         queries, "tp", split_axis=0, concat_axis=0, axis_index_groups=TP_GROUPS, tiled=True
     )
-    peers = 4
-    parts = pl.pallas_call(
-        attention_kernel,
-        grid=(TP // peers,),
-        in_specs=[
-            pl.BlockSpec(memory_space=pltpu.SMEM),
-            pl.BlockSpec((GROUP, peers * ROWS, HV), lambda i: (0, i, 0)),
-            whole_block((KEYS, 2 * HV)),
-            pl.BlockSpec((peers * ROWS, HV), lambda i: (i, 0)),
-        ],
-        out_specs=pl.BlockSpec((peers, MESSAGE, HV), lambda i: (i, 0, 0)),
-        out_shape=jax.ShapeDtypeStruct((TP, MESSAGE, HV), BF16),
-        compiler_params=params,
-        name="attention",
-    )(lambdas, queries, key_values, head_gate)
-    parts = lax.all_to_all(parts, "tp", split_axis=0, concat_axis=0, tiled=True)
+    first_parts = attend(queries, key_values, 0, params, (lambdas, head_gate))
+    first_parts = lax.all_to_all(first_parts, "tp", split_axis=0, concat_axis=0, tiled=True)
+    second_parts = attend(queries, key_values, 1, params, ())
+    second_parts = lax.all_to_all(second_parts, "tp", split_axis=0, concat_axis=0, tiled=True)
     mixed_out = pl.pallas_call(
         finish_kernel,
         grid=(TP // FINISH_PIECES,),
         in_specs=[
-            whole_block((TP, MESSAGE, HV)),
+            whole_block(first_parts.shape),
+            whole_block(second_parts.shape),
             pl.BlockSpec((2, FINISH_PIECES, GROUP * HV, D // TP), lambda i: (0, i, 0, 0)),
             whole_block((SP * TP, 1, CHUNK)),
             whole_block((1, D)),
@@ -334,7 +360,7 @@
         scratch_shapes=[pltpu.VMEM((ROWS, TP * HV), BF16), pltpu.VMEM((TP, ROWS, D // TP), F32)],
         compiler_params=params,
         name="finish",
-    )(parts, out_weights, sums, post_gain[None, :], head_gain[None, :])
+    )(first_parts, second_parts, out_weights, sums, post_gain[None, :], head_gain[None, :])
     return mixed_out[None]
 
 

time: 242 us -> 242 us (level)
  the two profiles are of different devices: /device:TPU:4 before, /device:TPU:2 now
where the time goes in v5:
time: 242 us
  waiting for transfers between devices  91.5 us (38%)
  starting transfers between devices  52.6 us (22%)
  blocking collectives  49.3 us (20%)
  Pallas kernels  29.1 us (12%)
  between operations  14.5 us (6%)
  other arithmetic  2.54 us (1%)
    all_gather x1, waiting for transfers between devices, compute(): halves = lax.all_gather(half, 'tp', axis=0, tiled=False)  39 us
    all_gather x1, blocking collectives, compute(): key_values = lax.all_gather(key_values, 'sp', axis=0, tiled=True)  30.1 us
    all_gather x1, waiting for transfers between devices, compute(): rows = lax.all_gather(latents[0], 'tp', axis=0, tiled=False)  24.4 us
    all_to_all x1, starting transfers between devices, compute(): lax.all_to_all(partials, both_axes, split_axis=0, concat_axis=0, tiled=True)  22 us
    all_to_all x1, blocking collectives, compute(): lax.all_to_all(first_parts, 'tp', split_axis=0, concat_axis=0, tiled=True)  19.2 us
    all_to_all x1, waiting for transfers between devices, compute(): lax.all_to_all(partials, both_axes, split_axis=0, concat_axis=0, tiled=True)  14.9 us
    pallas_call x2, Pallas kernels, attend(): pl.pallas_call(functools.partial(attention_kernel, bool(extra)), grid=(TP...  14.4 us
    all_to_all x1, starting transfers between devices, compute(): lax.all_to_all(copies, both_axes, split_axis=0, concat_axis=0, tiled=True)  14.3 us
  transfers between devices with their start and end apart: 8, of which 6 were waited for; matrix products, arithmetic and copies ran while one was open for 1% of the time, Pallas kernels for 9%

profile of v5, /device:TPU:2, one launch (start us, length us, event | category | flops | bytes accessed | tf_op | source)
XLA Modules:
  0.0 241.6 jit_solution(12043988380446925627)
XLA Ops:
  6.5 0.0 copy-start.3
  6.5 2.0 partial_sums.1
  8.6 22.0 %all-to-all-start = ((f32[96,1,256]{2,1,0:T(1,128)}), f32[96,1,256]{2,1,0:T(1,128)S(1)}, u32[]{:S(2)}, u32[]{:S(2)}) async-start(f32[96,1,256]{2,1,0:T(1,128)} %partial_sums.1), calls=%async_computation | async-start | bytes 196608 | tf_op jit(solution)/shard_map/all_to_all | solution.py:296
  30.6 0.0 all-gather.8.cloned.1.call-start
  30.6 14.9 %all-to-all-done = f32[96,1,256]{2,1,0:T(1,128)S(1)} async-done(((f32[96,1,256]{2,1,0:T(1,128)}), f32[96,1,256]{2,1,0:T(1,128)S(1)}, u32[]{:S(2)}, u32[]{:S(2)}) %all-to-all-start) | async-done | bytes 98336 | tf_op jit(solution)/shard_map/all_to_all | solution.py:296
  45.6 0.1 reduce_sum.9
  45.7 0.5 slice.4
  46.9 1.8 dynamic-slice_add_fusion
  48.7 0.0 all-gather.8.cloned.1.call-update
  48.7 0.0 all-gather.6.cloned.1.call-start
  48.7 0.7 all-gather.6.cloned.1.call-update
  49.5 0.0 all-gather.10.cloned.1.call-start
  49.5 39.0 %all-gather.8.cloned.1.call-done = bf16[4096,384]{1,0:T(8,128)(2,1)} async-done(((bf16[512,384]{1,0:T(8,128)(2,1)}), bf16[4096,384]{1,0:T(8,128)(2,1)}) %all-gather.8.cloned.1.call-update) | async-done | bytes 3145744 | tf_op jit(solution)/shard_map/all_gather | solution.py:302
  88.5 0.0 all-gather.10.cloned.1.call-update
  88.5 0.7 broadcast_in_dim.24
  89.2 14.3 %all-to-all-start.1 = ((f32[96,1,256]{2,1,0:T(1,128)}), f32[96,1,256]{2,1,0:T(1,128)S(1)}, u32[]{:S(2)}, u32[]{:S(2)}) async-start(f32[96,1,256]{2,1,0:T(1,128)} %broadcast_in_dim.24), calls=%async_computation.1 | async-start | bytes 196608 | tf_op jit(solution)/shard_map/all_to_all | solution.py:299
  103.5 0.0 copy-done.3
  103.5 7.2 %collective-permute-start = (bf16[4,3072]{1,0:T(4,128)(2,1)S(1)}, bf16[4,3072]{1,0:T(4,128)(2,1)S(1)}, u32[]{:S(2)}, u32[]{:S(2)}) collective-permute-start(bf16[4,3072]{1,0:T(4,128)(2,1)S(1)} %bitcast.15), channel_id=1, source_target_pairs={{0,32},{8,40},{16,48},{24,56},{32,0},{40,8},{48,16},{56,24},{1,33}... | collective-permute-start | bytes 73736 | tf_op jit(solution)/shard_map/ppermute | solution.py:287
  110.7 0.6 pad_add_fusion.place_ref
  111.3 2.7 %collective-permute-done.other_ref = bf16[4,3072]{1,0:T(4,128)(2,1)S(1)} collective-permute-done((bf16[4,3072]{1,0:T(4,128)(2,1)S(1)}, bf16[4,3072]{1,0:T(4,128)(2,1)S(1)}, u32[]{:S(2)}, u32[]{:S(2)}) %collective-permute-start) | collective-permute-done | bytes 24608 | tf_op jit(solution)/shard_map/ppermute | solution.py:287
  113.9 0.0 copy-start.4
  113.9 4.1 %all-to-all-done.1.sums_ref = f32[96,1,256]{2,1,0:T(1,128)S(1)} async-done(((f32[96,1,256]{2,1,0:T(1,128)}), f32[96,1,256]{2,1,0:T(1,128)S(1)}, u32[]{:S(2)}, u32[]{:S(2)}) %all-to-all-start.1) | async-done | bytes 98336 | tf_op jit(solution)/shard_map/all_to_all | solution.py:299
  118.0 0.0 copy-start.2
  118.0 24.4 %all-gather.6.cloned.1.call-done.rows_ref = bf16[8,64,3072]{2,1,0:T(8,128)(2,1)} async-done(((bf16[1,64,3072]{2,1,0:T(8,128)(2,1)}), bf16[8,64,3072]{2,1,0:T(8,128)(2,1)}) %all-gather.6.cloned.1.call-update) | async-done | bytes 3145744 | tf_op jit(solution)/shard_map/all_gather | solution.py:286
  142.4 0.0 copy-done.4
  142.4 0.0 copy-done.2
  142.4 6.5 %project.1 = (bf16[4,512,128]{2,1,0:T(8,128)(2,1)}, bf16[512,128]{1,0:T(8,128)(2,1)}, bf16[136,256]{1,0:T(8,128)(2,1)}) custom-call(s32[2]{0:T(128)} %pad_add_fusion.place_ref, bf16[8,64,3072]{2,1,0:T(8,128)(2,1)} %all-gather.6.cloned.1.call-done.rows_ref, bf16[4,3072]{1,0:T(4,128)(2,1)} %bitcast.14, bf16[4,3072]{1,0:T(4,128)(2,1)} %copy-done.4, ...), custom_call_target="tpu_custom_call" | custom-call | tf_op jit(solution)/shard_map/project/pallas_call | solution.py:305
  148.8 4.0 %all-to-all-start.2 = ((bf16[4,512,128]{2,1,0:T(8,128)(2,1)}), bf16[4,512,128]{2,1,0:T(8,128)(2,1)S(1)}, u32[]{:S(2)}, u32[]{:S(2)}) async-start(bf16[4,512,128]{2,1,0:T(8,128)(2,1)} %get-tuple-element.9), calls=%async_computation.2 | async-start | bytes 1048576 | tf_op jit(solution)/shard_map/all_to_all | solution.py:340
  152.8 30.1 %all_gather.19.refs_3_.refs_1_ = bf16[1632,256]{1,0:T(8,128)(2,1)} all-gather(bf16[136,256]{1,0:T(8,128)(2,1)} %get-tuple-element.10), channel_id=1, replica_groups=mesh['sp'=12,'tp'=8,'dp'=8] {'sp'}, dimensions={0}, use_global_device_ids=true | all-gather | bytes 905216 | tf_op jit(solution)/shard_map/all_gather | solution.py:339
  182.9 0.0 all-to-all-done.2.refs_2_.refs_0_
  182.9 0.0 copy-start
  182.9 0.8 copy-done
  183.7 7.1 %attention.3 = bf16[8,272,128]{2,1,0:T(8,128)(2,1)} custom-call(bf16[4,512,128]{2,1,0:T(8,128)(2,1)} %copy-done, bf16[1632,256]{1,0:T(8,128)(2,1)} %all_gather.19.refs_3_.refs_1_), custom_call_target="tpu_custom_call" | custom-call | tf_op jit(solution)/shard_map/attention/pallas_call | solution.py:262
  190.8 5.1 %all-to-all-start.4 = ((bf16[8,272,128]{2,1,0:T(8,128)(2,1)}), bf16[8,272,128]{2,1,0:T(8,128)(2,1)S(1)}, u32[]{:S(2)}, u32[]{:S(2)}) async-start(bf16[8,272,128]{2,1,0:T(8,128)(2,1)} %attention.3), calls=%async_computation.4 | async-start | bytes 1114112 | tf_op jit(solution)/shard_map/all_to_all | solution.py:346
  196.6 7.2 %attention.2 = bf16[8,336,128]{2,1,0:T(8,128)(2,1)} custom-call(f32[1]{0:T(128)S(6)} %copy.17.refs_0_, bf16[512,128]{1,0:T(8,128)(2,1)} %get-tuple-element.8.refs_1_, bf16[4,512,128]{2,1,0:T(8,128)(2,1)} %copy-done, bf16[1632,256]{1,0:T(8,128)(2,1)} %all_gather.19.refs_3_.refs_1_), custom_call_target="tpu_custom_call" | custom-call | tf_op jit(solution)/shard_map/attention/pallas_call | solution.py:262
  203.8 5.8 %all-to-all-done.4.second_ref = bf16[8,272,128]{2,1,0:T(8,128)(2,1)S(1)} async-done(((bf16[8,272,128]{2,1,0:T(8,128)(2,1)}), bf16[8,272,128]{2,1,0:T(8,128)(2,1)S(1)}, u32[]{:S(2)}, u32[]{:S(2)}) %all-to-all-start.4) | async-done | bytes 557088 | tf_op jit(solution)/shard_map/all_to_all | solution.py:346
  209.6 0.0 copy-start.1
  209.6 19.2 %all_to_all.25.first_ref = bf16[8,336,128]{2,1,0:T(8,128)(2,1)} all-to-all(bf16[8,336,128]{2,1,0:T(8,128)(2,1)} %attention.2), channel_id=1, replica_groups=mesh['sp'=12,'tp'=8,'dp'=8] {'tp'}, dimensions={0} | all-to-all | bytes 1376256 | tf_op jit(solution)/shard_map/all_to_all | solution.py:344
  228.8 0.0 all-gather.10.cloned.1.call-done
  228.8 0.0 copy-done.1
  228.8 6.2 %finish.1 = bf16[64,3072]{1,0:T(8,128)(2,1)} custom-call(bf16[8,336,128]{2,1,0:T(8,128)(2,1)} %all_to_all.25.first_ref, bf16[8,272,128]{2,1,0:T(8,128)(2,1)} %copy-done.1, bf16[2,8,512,384]{3,2,1,0:T(8,128)(2,1)} %bitcast.12, f32[96,1,256]{2,1,0:T(1,128)} %copy-done.2, f32[1,3072]{1,0:T(1,128)} %bitcast.17, f32[1,128]{1,0:T(1,128)} %bitcast.19), custom_call_target="tpu_custom_call" | custom-call | tf_op jit(solution)/shard_map/finish/pallas_call | solution.py:347
Async XLA Ops:
  6.5 96.9 %copy-start.3 = (bf16[1,4,3072]{2,1,0:T(4,128)(2,1)S(1)}, bf16[1,4,3072]{2,1,0:T(4,128)(2,1)}, u32[]{:S(2)}) copy-start(bf16[1,4,3072]{2,1,0:T(4,128)(2,1)} %param.18) | copy-start | bytes 73732
  8.6 37.0 %all-to-all-start = ((f32[96,1,256]{2,1,0:T(1,128)}), f32[96,1,256]{2,1,0:T(1,128)S(1)}, u32[]{:S(2)}, u32[]{:S(2)}) async-start(f32[96,1,256]{2,1,0:T(1,128)} %partial_sums.1), calls=%async_computation | async-start | bytes 196608 | tf_op jit(solution)/shard_map/all_to_all | solution.py:296
  30.6 57.9 %all-gather.8.cloned.1.call-start = ((), (), s32[]{:S(2)}) async-start(), calls=%async_computation.6 | async-start | bytes 3538944 | tf_op jit(solution)/shard_map/all_gather | solution.py:302
  48.7 93.7 %all-gather.6.cloned.1.call-start = ((), (), s32[]{:S(2)}) async-start(), calls=%async_computation.5 | async-start | bytes 3538944 | tf_op jit(solution)/shard_map/all_gather | solution.py:286
  49.5 179.3 %all-gather.10.cloned.1.call-start = ((), (), s32[]{:S(2)}) async-start(), calls=%async_computation.7 | async-start | bytes 9437184 | tf_op jit(solution)/shard_map/all_gather | solution.py:303
  89.2 28.8 %all-to-all-start.1 = ((f32[96,1,256]{2,1,0:T(1,128)}), f32[96,1,256]{2,1,0:T(1,128)S(1)}, u32[]{:S(2)}, u32[]{:S(2)}) async-start(f32[96,1,256]{2,1,0:T(1,128)} %broadcast_in_dim.24), calls=%async_computation.1 | async-start | bytes 196608 | tf_op jit(solution)/shard_map/all_to_all | solution.py:299
  103.5 10.5 %collective-permute-start = (bf16[4,3072]{1,0:T(4,128)(2,1)S(1)}, bf16[4,3072]{1,0:T(4,128)(2,1)S(1)}, u32[]{:S(2)}, u32[]{:S(2)}) collective-permute-start(bf16[4,3072]{1,0:T(4,128)(2,1)S(1)} %bitcast.15), channel_id=1, source_target_pairs={{0,32},{8,40},{16,48},{24,56},{32,0},{40,8},{48,16},{56,24},{1,33}... | collective-permute-start | bytes 73736 | tf_op jit(solution)/shard_map/ppermute | solution.py:287
  113.9 28.4 %copy-start.4 = (bf16[4,3072]{1,0:T(4,128)(2,1)}, bf16[4,3072]{1,0:T(4,128)(2,1)S(1)}, u32[]{:S(2)}) copy-start(bf16[4,3072]{1,0:T(4,128)(2,1)S(1)} %collective-permute-done.other_ref) | copy-start | bytes 73732
  118.0 24.4 %copy-start.2 = (f32[96,1,256]{2,1,0:T(1,128)}, f32[96,1,256]{2,1,0:T(1,128)S(1)}, u32[]{:S(2)}) copy-start(f32[96,1,256]{2,1,0:T(1,128)S(1)} %all-to-all-done.1.sums_ref) | copy-start | bytes 294916
  148.8 34.1 %all-to-all-start.2 = ((bf16[4,512,128]{2,1,0:T(8,128)(2,1)}), bf16[4,512,128]{2,1,0:T(8,128)(2,1)S(1)}, u32[]{:S(2)}, u32[]{:S(2)}) async-start(bf16[4,512,128]{2,1,0:T(8,128)(2,1)} %get-tuple-element.9), calls=%async_computation.2 | async-start | bytes 1048576 | tf_op jit(solution)/shard_map/all_to_all | solution.py:340
  182.9 0.8 copy-start
  190.8 18.7 %all-to-all-start.4 = ((bf16[8,272,128]{2,1,0:T(8,128)(2,1)}), bf16[8,272,128]{2,1,0:T(8,128)(2,1)S(1)}, u32[]{:S(2)}, u32[]{:S(2)}) async-start(bf16[8,272,128]{2,1,0:T(8,128)(2,1)} %attention.3), calls=%async_computation.4 | async-start | bytes 1114112 | tf_op jit(solution)/shard_map/all_to_all | solution.py:346
  209.6 19.2 %copy-start.1 = (bf16[8,272,128]{2,1,0:T(8,128)(2,1)}, bf16[8,272,128]{2,1,0:T(8,128)(2,1)S(1)}, u32[]{:S(2)}) copy-start(bf16[8,272,128]{2,1,0:T(8,128)(2,1)S(1)} %all-to-all-done.4.second_ref) | copy-start | bytes 1671172
Sparse Core Ops, SparseCore 0:
  48.8 39.6 all-gather.7
  90.8 51.4 all-gather.5
  144.7 25.1 all-gather.9

commit v6 on v5

--- a/solution.py
+++ b/solution.py
@@ -32,7 +32,6 @@
 F32 = jnp.float32
 BF16 = jnp.bfloat16
 TP_GROUPS = [[0, 1, 2, 3], [4, 5, 6, 7]]
-CORE_PAIRS = [[0, 1], [2, 3], [4, 5], [6, 7]]
 VMEM_LIMIT = 60 * 1024 * 1024
 
 
@@ -178,7 +177,7 @@
 
 
 def finish_kernel(
-    first_ref, second_ref, weight_ref, sums_ref, post_gain_ref, head_gain_ref,
+    core_ref, first_ref, second_ref, own_ref, other_ref, sums_ref, post_gain_ref, head_gain_ref,
     out_ref, branch_ref, projected_ref,
 ):
     step = pl.program_id(0)
@@ -227,12 +226,15 @@
             square = jnp.mean(attended * attended, axis=-1, keepdims=True)
             gate = first_ref[head, GATE_ROW : GATE_ROW + ROWS, :].astype(F32)
             branch = attended * lax.rsqrt(square + NORM_EPSILON) * head_gain_ref[...] * silu(gate)
-            branch_ref[:, head * HV : (head + 1) * HV] = branch.astype(BF16)
-
-    pieces = weight_ref.shape[1]
+            branch_ref[g, :, j * HV : (j + 1) * HV] = branch.astype(BF16)
+
+    own = core_ref[0]
+    pieces = own_ref.shape[0]
     for piece in range(pieces):
-        weight = weight_ref[:, piece].reshape(TP * HV, D // TP)
-        projected = jnp.dot(branch_ref[...], weight, preferred_element_type=F32)
+        projected = jnp.dot(branch_ref[own], own_ref[piece], preferred_element_type=F32)
+        projected = projected + jnp.dot(
+            branch_ref[1 - own], other_ref[piece], preferred_element_type=F32
+        )
         projected_ref[step * pieces + piece] = projected.astype(BF16).astype(F32)
 
     @pl.when(step == pl.num_programs(0) - 1)
@@ -299,8 +301,8 @@
     sums = lax.all_to_all(copies, both_axes, split_axis=0, concat_axis=0, tiled=True)
     half = lax.dynamic_slice_in_dim(out_weight, core * GROUP * HV, GROUP * HV, 0)
     half = half + (own_sums[0, 0, 0] * 0.0).astype(BF16)
-    halves = lax.all_gather(half, "tp", axis=0, tiled=False)
-    out_weights = lax.all_gather(halves, "dp", axis=0, tiled=False, axis_index_groups=CORE_PAIRS)
+    own_half = lax.all_gather(half, "tp", axis=0, tiled=False)
+    other_half = lax.ppermute(own_half, "dp", [(i, i ^ 1) for i in range(8)])
     place = jnp.stack([t % GROUP, t // GROUP]).astype(jnp.int32)
     queries, head_gate, key_values = pl.pallas_call(
         project_kernel,
@@ -344,23 +346,34 @@
     first_parts = lax.all_to_all(first_parts, "tp", split_axis=0, concat_axis=0, tiled=True)
     second_parts = attend(queries, key_values, 1, params, ())
     second_parts = lax.all_to_all(second_parts, "tp", split_axis=0, concat_axis=0, tiled=True)
+    weight_block = pl.BlockSpec((FINISH_PIECES, GROUP * HV, D // TP), lambda i, _: (i, 0, 0))
     mixed_out = pl.pallas_call(
         finish_kernel,
-        grid=(TP // FINISH_PIECES,),
-        in_specs=[
-            whole_block(first_parts.shape),
-            whole_block(second_parts.shape),
-            pl.BlockSpec((2, FINISH_PIECES, GROUP * HV, D // TP), lambda i: (0, i, 0, 0)),
-            whole_block((SP * TP, 1, CHUNK)),
-            whole_block((1, D)),
-            whole_block((1, HV)),
-        ],
-        out_specs=whole_block((ROWS, D)),
+        grid_spec=pltpu.PrefetchScalarGridSpec(
+            num_scalar_prefetch=1,
+            grid=(TP // FINISH_PIECES,),
+            in_specs=[
+                whole_block(first_parts.shape),
+                whole_block(second_parts.shape),
+                weight_block,
+                weight_block,
+                whole_block((SP * TP, 1, CHUNK)),
+                whole_block((1, D)),
+                whole_block((1, HV)),
+            ],
+            out_specs=whole_block((ROWS, D)),
+            scratch_shapes=[
+                pltpu.VMEM((2, ROWS, GROUP * HV), BF16),
+                pltpu.VMEM((TP, ROWS, D // TP), F32),
+            ],
+        ),
         out_shape=jax.ShapeDtypeStruct((ROWS, D), BF16),
-        scratch_shapes=[pltpu.VMEM((ROWS, TP * HV), BF16), pltpu.VMEM((TP, ROWS, D // TP), F32)],
         compiler_params=params,
         name="finish",
-    )(first_parts, second_parts, out_weights, sums, post_gain[None, :], head_gain[None, :])
+    )(
+        core.astype(jnp.int32)[None], first_parts, second_parts, own_half, other_half, sums,
+        post_gain[None, :], head_gain[None, :],
+    )
     return mixed_out[None]
 
 

time: 242 us -> 243 us (level)
  starting transfers between devices: 52.6 us -> 44 us
  waiting for transfers between devices: 91.5 us -> 99 us
    all_gather x1, waiting for transfers between devices: 24.4 us -> 38.9 us  [compute(): rows = lax.all_gather(latents[0], 'tp', axis=0, tiled=False)]
    all_to_all x1, starting transfers between devices: 14.3 us -> 5.87 us  [compute(): lax.all_to_all(copies, both_axes, split_axis=0, concat_axis=0, tiled=True)]
    all_gather x2 -> x1, waiting for transfers between devices: 39 us -> 34.4 us  [compute(): own_half = lax.all_gather(half, 'tp', axis=0, tiled=False)]
    all_to_all x1, waiting for transfers between devices: 4.06 us -> 0.01 us  [compute(): lax.all_to_all(copies, both_axes, split_axis=0, concat_axis=0, tiled=True)]
  transfers between devices with their start and end apart: 8 -> 8, of which waited for: 6 -> 5; matrix products, arithmetic and copies ran while one was open for 1% -> 1% of each run, Pallas kernels for 9% -> 9%
where the time goes in v6:
time: 243 us; the launch traced here: 242 us
  waiting for transfers between devices  99 us (41%)
  blocking collectives  50.8 us (21%)
  starting transfers between devices  44 us (18%)
  Pallas kernels  29.1 us (12%)
  between operations  14.8 us (6%)
  other arithmetic  2.5 us (1%)
    all_gather x1, waiting for transfers between devices, compute(): rows = lax.all_gather(latents[0], 'tp', axis=0, tiled=False)  38.9 us
    all_gather x1, waiting for transfers between devices, compute(): own_half = lax.all_gather(half, 'tp', axis=0, tiled=False)  34.4 us
    all_gather x1, blocking collectives, compute(): key_values = lax.all_gather(key_values, 'sp', axis=0, tiled=True)  31.5 us
    all_to_all x1, starting transfers between devices, compute(): lax.all_to_all(partials, both_axes, split_axis=0, concat_axis=0, tiled=True)  22 us
    all_to_all x1, blocking collectives, compute(): lax.all_to_all(first_parts, 'tp', split_axis=0, concat_axis=0, tiled=True)  19.2 us
    all_to_all x1, waiting for transfers between devices, compute(): lax.all_to_all(partials, both_axes, split_axis=0, concat_axis=0, tiled=True)  14.9 us
    pallas_call x2, Pallas kernels, attend(): pl.pallas_call(functools.partial(attention_kernel, bool(extra)), grid=(TP...  14.4 us
    pallas_call x1, Pallas kernels, compute(): pl.pallas_call(project_kernel, grid_spec=pltpu.PrefetchScalarGridSpec(num...  6.43 us
  transfers between devices with their start and end apart: 8, of which 5 were waited for; matrix products, arithmetic and copies ran while one was open for 1% of the time, Pallas kernels for 9%

profile of v6, /device:TPU:2, one launch (start us, length us, event | category | flops | bytes accessed | tf_op | source)
XLA Modules:
  0.0 242.2 jit_solution(16339969383907816105)
XLA Ops:
  6.5 2.0 partial_sums.1
  8.6 22.0 %all-to-all-start = ((f32[96,1,256]{2,1,0:T(1,128)}), f32[96,1,256]{2,1,0:T(1,128)S(1)}, u32[]{:S(2)}, u32[]{:S(2)}) async-start(f32[96,1,256]{2,1,0:T(1,128)} %partial_sums.1), calls=%async_computation | async-start | bytes 196608 | tf_op jit(solution)/shard_map/all_to_all | solution.py:298
  30.6 0.0 all-gather.6.cloned.1.call-start
  30.6 14.9 %all-to-all-done = f32[96,1,256]{2,1,0:T(1,128)S(1)} async-done(((f32[96,1,256]{2,1,0:T(1,128)}), f32[96,1,256]{2,1,0:T(1,128)S(1)}, u32[]{:S(2)}, u32[]{:S(2)}) %all-to-all-start) | async-done | bytes 98336 | tf_op jit(solution)/shard_map/all_to_all | solution.py:298
  45.6 0.1 reduce_sum.9
  45.7 0.5 slice.4
  46.8 1.8 dynamic-slice_add_fusion
  48.7 0.0 all-gather.6.cloned.1.call-update
  48.7 0.0 all-gather.4.cloned.1.call-start
  48.7 0.7 all-gather.4.cloned.1.call-update
  49.4 0.7 broadcast_in_dim.28
  50.1 5.9 %all-to-all-start.1 = ((f32[96,1,256]{2,1,0:T(1,128)}), f32[96,1,256]{2,1,0:T(1,128)S(1)}, u32[]{:S(2)}, u32[]{:S(2)}) async-start(f32[96,1,256]{2,1,0:T(1,128)} %broadcast_in_dim.28), calls=%async_computation.1 | async-start | bytes 196608 | tf_op jit(solution)/shard_map/all_to_all | solution.py:301
  56.0 34.4 %all-gather.6.cloned.1.call-done = bf16[4096,384]{1,0:T(8,128)(2,1)} async-done(((bf16[512,384]{1,0:T(8,128)(2,1)}), bf16[4096,384]{1,0:T(8,128)(2,1)}) %all-gather.6.cloned.1.call-update) | async-done | bytes 3145744 | tf_op jit(solution)/shard_map/all_gather | solution.py:304
  90.4 1.9 collective-permute-start.1
  92.3 5.0 %collective-permute-start = (bf16[4,3072]{1,0:T(4,128)(2,1)}, bf16[4,3072]{1,0:T(4,128)(2,1)S(1)}, u32[]{:S(2)}, u32[]{:S(2)}) collective-permute-start(bf16[4,3072]{1,0:T(4,128)(2,1)} %bitcast.14), channel_id=1, source_target_pairs={{0,32},{8,40},{16,48},{24,56},{32,0},{40,8},{48,16},{56,24},{1,33}... | collective-permute-start | bytes 73736 | tf_op jit(solution)/shard_map/ppermute | solution.py:289
  97.3 0.6 pad_add_fusion.place_ref
  97.9 4.3 %collective-permute-done.other_ref = bf16[4,3072]{1,0:T(4,128)(2,1)S(1)} collective-permute-done((bf16[4,3072]{1,0:T(4,128)(2,1)}, bf16[4,3072]{1,0:T(4,128)(2,1)S(1)}, u32[]{:S(2)}, u32[]{:S(2)}) %collective-permute-start) | collective-permute-done | bytes 24608 | tf_op jit(solution)/shard_map/ppermute | solution.py:289
  102.1 0.0 copy-start.3
  102.1 0.0 all-to-all-done.1.sums_ref
  102.1 0.0 copy-start.2
  102.1 38.9 %all-gather.4.cloned.1.call-done.rows_ref = bf16[8,64,3072]{2,1,0:T(8,128)(2,1)} async-done(((bf16[1,64,3072]{2,1,0:T(8,128)(2,1)}), bf16[8,64,3072]{2,1,0:T(8,128)(2,1)}) %all-gather.4.cloned.1.call-update) | async-done | bytes 3145744 | tf_op jit(solution)/shard_map/all_gather | solution.py:288
  141.1 0.0 copy-done.3
  141.1 0.0 copy-done.2
  141.1 6.4 %project.1 = (bf16[4,512,128]{2,1,0:T(8,128)(2,1)}, bf16[512,128]{1,0:T(8,128)(2,1)}, bf16[136,256]{1,0:T(8,128)(2,1)}) custom-call(s32[2]{0:T(128)} %pad_add_fusion.place_ref, bf16[8,64,3072]{2,1,0:T(8,128)(2,1)} %all-gather.4.cloned.1.call-done.rows_ref, bf16[4,3072]{1,0:T(4,128)(2,1)} %bitcast.15, bf16[4,3072]{1,0:T(4,128)(2,1)} %copy-done.3, ...), custom_call_target="tpu_custom_call" | custom-call | tf_op jit(solution)/shard_map/project/pallas_call | solution.py:307
  147.5 4.2 %all-to-all-start.2 = ((bf16[4,512,128]{2,1,0:T(8,128)(2,1)}), bf16[4,512,128]{2,1,0:T(8,128)(2,1)S(1)}, u32[]{:S(2)}, u32[]{:S(2)}) async-start(bf16[4,512,128]{2,1,0:T(8,128)(2,1)} %get-tuple-element.9), calls=%async_computation.2 | async-start | bytes 1048576 | tf_op jit(solution)/shard_map/all_to_all | solution.py:342
  151.7 31.5 %all_gather.13.refs_3_.refs_1_ = bf16[1632,256]{1,0:T(8,128)(2,1)} all-gather(bf16[136,256]{1,0:T(8,128)(2,1)} %get-tuple-element.10), channel_id=1, replica_groups=mesh['sp'=12,'tp'=8,'dp'=8] {'sp'}, dimensions={0}, use_global_device_ids=true | all-gather | bytes 905216 | tf_op jit(solution)/shard_map/all_gather | solution.py:341
  183.2 0.0 all-to-all-done.2.refs_2_.refs_0_
  183.2 0.0 copy-start
  183.2 0.8 copy-done
  184.1 7.2 %attention.3 = bf16[8,272,128]{2,1,0:T(8,128)(2,1)} custom-call(bf16[4,512,128]{2,1,0:T(8,128)(2,1)} %copy-done, bf16[1632,256]{1,0:T(8,128)(2,1)} %all_gather.13.refs_3_.refs_1_), custom_call_target="tpu_custom_call" | custom-call | tf_op jit(solution)/shard_map/attention/pallas_call | solution.py:264
  191.3 5.0 %all-to-all-start.4 = ((bf16[8,272,128]{2,1,0:T(8,128)(2,1)}), bf16[8,272,128]{2,1,0:T(8,128)(2,1)S(1)}, u32[]{:S(2)}, u32[]{:S(2)}) async-start(bf16[8,272,128]{2,1,0:T(8,128)(2,1)} %attention.3), calls=%async_computation.4 | async-start | bytes 1114112 | tf_op jit(solution)/shard_map/all_to_all | solution.py:348
  196.9 7.2 %attention.2 = bf16[8,336,128]{2,1,0:T(8,128)(2,1)} custom-call(f32[1]{0:T(128)S(6)} %copy.17.refs_0_, bf16[512,128]{1,0:T(8,128)(2,1)} %get-tuple-element.8.refs_1_, bf16[4,512,128]{2,1,0:T(8,128)(2,1)} %copy-done, bf16[1632,256]{1,0:T(8,128)(2,1)} %all_gather.13.refs_3_.refs_1_), custom_call_target="tpu_custom_call" | custom-call | tf_op jit(solution)/shard_map/attention/pallas_call | solution.py:264
  204.1 5.8 %all-to-all-done.4.second_ref = bf16[8,272,128]{2,1,0:T(8,128)(2,1)S(1)} async-done(((bf16[8,272,128]{2,1,0:T(8,128)(2,1)}), bf16[8,272,128]{2,1,0:T(8,128)(2,1)S(1)}, u32[]{:S(2)}, u32[]{:S(2)}) %all-to-all-start.4) | async-done | bytes 557088 | tf_op jit(solution)/shard_map/all_to_all | solution.py:348
  209.9 0.0 copy-start.1
  209.9 19.2 %all_to_all.25.first_ref = bf16[8,336,128]{2,1,0:T(8,128)(2,1)} all-to-all(bf16[8,336,128]{2,1,0:T(8,128)(2,1)} %attention.2), channel_id=1, replica_groups=mesh['sp'=12,'tp'=8,'dp'=8] {'tp'}, dimensions={0} | all-to-all | bytes 1376256 | tf_op jit(solution)/shard_map/all_to_all | solution.py:346
  229.1 0.0 collective-permute-done.1.other_ref
  229.1 0.0 copy-done.1
  229.1 6.2 %finish.1 = bf16[64,3072]{1,0:T(8,128)(2,1)} custom-call(s32[1]{0:T(128)} %bitcast.core_ref, bf16[8,336,128]{2,1,0:T(8,128)(2,1)} %all_to_all.25.first_ref, bf16[8,272,128]{2,1,0:T(8,128)(2,1)} %copy-done.1, bf16[8,512,384]{2,1,0:T(8,128)(2,1)} %bitcast.13, bf16[8,512,384]{2,1,0:T(8,128)(2,1)} %collective-permute-done.1.other_ref, f32[96,1,256]{2,1,0:T(1,128)} %copy-done.2, ...), custom_call_target="tpu_custom_call" | custom-call | tf_op jit(solution)/shard_map/finish/pallas_call | solution.py:350
Async XLA Ops:
  8.6 37.0 %all-to-all-start = ((f32[96,1,256]{2,1,0:T(1,128)}), f32[96,1,256]{2,1,0:T(1,128)S(1)}, u32[]{:S(2)}, u32[]{:S(2)}) async-start(f32[96,1,256]{2,1,0:T(1,128)} %partial_sums.1), calls=%async_computation | async-start | bytes 196608 | tf_op jit(solution)/shard_map/all_to_all | solution.py:298
  30.6 59.8 %all-gather.6.cloned.1.call-start = ((), (), s32[]{:S(2)}) async-start(), calls=%async_computation.6 | async-start | bytes 3538944 | tf_op jit(solution)/shard_map/all_gather | solution.py:304
  48.7 92.4 %all-gather.4.cloned.1.call-start = ((), (), s32[]{:S(2)}) async-start(), calls=%async_computation.5 | async-start | bytes 3538944 | tf_op jit(solution)/shard_map/all_gather | solution.py:288
  50.1 52.0 %all-to-all-start.1 = ((f32[96,1,256]{2,1,0:T(1,128)}), f32[96,1,256]{2,1,0:T(1,128)S(1)}, u32[]{:S(2)}, u32[]{:S(2)}) async-start(f32[96,1,256]{2,1,0:T(1,128)} %broadcast_in_dim.28), calls=%async_computation.1 | async-start | bytes 196608 | tf_op jit(solution)/shard_map/all_to_all | solution.py:301
  90.4 138.7 %collective-permute-start.1 = (bf16[8,512,384]{2,1,0:T(8,128)(2,1)}, bf16[8,512,384]{2,1,0:T(8,128)(2,1)}, u32[]{:S(2)}, u32[]{:S(2)}) collective-permute-start(bf16[8,512,384]{2,1,0:T(8,128)(2,1)} %bitcast.12), channel_id=1, source_target_pairs={{0,1},{1,0},{2,3},{3,2},{4,5},{5,4},{6,7},{7,6},{8,9},{9,8},{10,11... | collective-permute-start | bytes 9437192 | tf_op jit(solution)/shard_map/ppermute | solution.py:305
  92.3 9.8 %collective-permute-start = (bf16[4,3072]{1,0:T(4,128)(2,1)}, bf16[4,3072]{1,0:T(4,128)(2,1)S(1)}, u32[]{:S(2)}, u32[]{:S(2)}) collective-permute-start(bf16[4,3072]{1,0:T(4,128)(2,1)} %bitcast.14), channel_id=1, source_target_pairs={{0,32},{8,40},{16,48},{24,56},{32,0},{40,8},{48,16},{56,24},{1,33}... | collective-permute-start | bytes 73736 | tf_op jit(solution)/shard_map/ppermute | solution.py:289
  102.1 39.0 %copy-start.3 = (bf16[4,3072]{1,0:T(4,128)(2,1)}, bf16[4,3072]{1,0:T(4,128)(2,1)S(1)}, u32[]{:S(2)}) copy-start(bf16[4,3072]{1,0:T(4,128)(2,1)S(1)} %collective-permute-done.other_ref) | copy-start | bytes 73732
  102.1 39.0 %copy-start.2 = (f32[96,1,256]{2,1,0:T(1,128)}, f32[96,1,256]{2,1,0:T(1,128)S(1)}, u32[]{:S(2)}) copy-start(f32[96,1,256]{2,1,0:T(1,128)S(1)} %all-to-all-done.1.sums_ref) | copy-start | bytes 294916
  147.5 35.7 %all-to-all-start.2 = ((bf16[4,512,128]{2,1,0:T(8,128)(2,1)}), bf16[4,512,128]{2,1,0:T(8,128)(2,1)S(1)}, u32[]{:S(2)}, u32[]{:S(2)}) async-start(bf16[4,512,128]{2,1,0:T(8,128)(2,1)} %get-tuple-element.9), calls=%async_computation.2 | async-start | bytes 1048576 | tf_op jit(solution)/shard_map/all_to_all | solution.py:342
  183.2 0.8 copy-start
  191.3 18.6 %all-to-all-start.4 = ((bf16[8,272,128]{2,1,0:T(8,128)(2,1)}), bf16[8,272,128]{2,1,0:T(8,128)(2,1)S(1)}, u32[]{:S(2)}, u32[]{:S(2)}) async-start(bf16[8,272,128]{2,1,0:T(8,128)(2,1)} %attention.3), calls=%async_computation.4 | async-start | bytes 1114112 | tf_op jit(solution)/shard_map/all_to_all | solution.py:348
  209.9 19.2 %copy-start.1 = (bf16[8,272,128]{2,1,0:T(8,128)(2,1)}, bf16[8,272,128]{2,1,0:T(8,128)(2,1)S(1)}, u32[]{:S(2)}) copy-start(bf16[8,272,128]{2,1,0:T(8,128)(2,1)S(1)} %all-to-all-done.4.second_ref) | copy-start | bytes 1671172
Sparse Core Ops, SparseCore 0:
  48.8 41.5 all-gather.5
  92.7 48.3 all-gather.3
